TPU v7x, 128 devices: a whole 4x4x4 slice. The times are simulated.
128 devices in a mesh: sp: 32 (over z, y, core), tp: 4 (over x).
Axes of the slice: x: 4, y: 4, z: 4, core: 2. Of those that a mesh axis runs over, the one named last changes fastest.
Arguments:
- resid: bfloat16 [8192, 2048], P(('sp', 'tp')), may hold values from -0.21875 to 0.21875
- query_a: bfloat16 [8192, 1024], P('sp', 'tp'), may hold values from -6 to 6
- key_a: bfloat16 [8192, 256], P('sp', 'tp'), may hold values from -6 to 6
- value_a: bfloat16 [8192, 256], P('sp', 'tp'), may hold values from -6 to 6
- query_b: bfloat16 [8192, 1024], P('sp', 'tp'), may hold values from -6 to 6
- key_b: bfloat16 [8192, 512], P('sp', 'tp'), may hold values from -6 to 6
- value_b: bfloat16 [8192, 512], P('sp', 'tp'), may hold values from -6 to 6
- gain_qa: float32 [64], replicated, may hold values from 0.1 to 8
- gain_ka: float32 [64], replicated, may hold values from 0.1 to 8
- gain_qb: float32 [128], replicated, may hold values from 0.1 to 8
- gain_kb: float32 [128], replicated, may hold values from 0.1 to 8
- w_out_a: bfloat16 [1024, 2048], P('tp'), may hold values from -0.125 to 0.125
- w_out_b: bfloat16 [1024, 2048], P('tp'), may hold values from -0.125 to 0.125
- norm_gain: float32 [2048], replicated, may hold values from 0.1 to 1.9
- w_up: bfloat16 [2048, 8192], P('sp', 'tp'), may hold values from -0.125 to 0.125
- w_down: bfloat16 [8192, 2048], P('tp', 'sp'), may hold values from -0.0625 to 0.0625
Outputs:
- result: bfloat16 [8192, 2048], P(('sp', 'tp'))
All inputs are finite; a program needn't handle non-finite values.
Results may differ from a plain program's by a relative error of at most 0.02.
The roundings to bfloat16 on the way count: a program that leaves them out, or rounds other values in their place, can miss the bound.
Values may be sent and summed in bfloat16 or wider, within the bound.
A program may use at most 128 MiB of HBM per device.

v0:
```python
import math

import jax
import jax.numpy as jnp
from jax import lax
from jax.sharding import PartitionSpec as P

GRID_W = 64


EPS = 1e-06


def side_by_side(arrays, axis, dim, along):
    both = jnp.concatenate(arrays, axis=along)
    result, at, outs = (lax.all_gather(both, axis, axis=dim, tiled=True), 0, [])
    for a in arrays:
        outs.append(lax.slice_in_dim(result, at, at + a.shape[along], axis=along))
        at += a.shape[along]
    return tuple(outs)


def split_up(shard, dim, length):
    dims = shard.shape
    blocks = shard.reshape(*dims[:dim], length, dims[dim] // length, *dims[dim + 1 :])
    return jnp.moveaxis(blocks, dim, 0)


def sum_at_owner(shard, axis, dim):
    length = lax.axis_size(axis)
    blocks = lax.all_to_all(split_up(shard, dim, length), axis, 0, 0, tiled=True)
    return jnp.sum(blocks.astype(jnp.float32), axis=0)


def copy_for_each(shard, axis):
    length = lax.axis_size(axis)
    return lax.all_to_all(
        jnp.broadcast_to(shard[None], (length, *shard.shape)), axis, 0, 0, tiled=True
    )


def in_order(blocks, dim):
    dims = list(blocks.shape[1:])
    dims[dim] *= blocks.shape[0]
    return jnp.moveaxis(blocks, 0, dim).reshape(dims)


def gather_directly(shard, axis, dim):
    blocks = copy_for_each(shard, axis)
    return in_order(blocks, dim)


def norm_rope(values, gain, places):
    width = gain.shape[0]
    count = values.shape[0]
    flat = values.astype(jnp.float32).reshape(count, -1, width)
    flat = flat * lax.rsqrt(jnp.mean(flat * flat, axis=-1, keepdims=True) + EPS) * gain
    grid_rows = (places // GRID_W).astype(jnp.float32)
    grid_cols = (places % GRID_W).astype(jnp.float32)
    quarter = width // 4
    freqs = 10000.0 ** (-(2.0 * jnp.arange(quarter, dtype=jnp.float32)) / (width // 2))
    ang_r = grid_rows[:, None] * freqs
    ang_c = grid_cols[:, None] * freqs
    angles = jnp.concatenate([ang_r, ang_r, ang_c, ang_c], axis=-1)
    one, two, three, four = jnp.split(flat, 4, axis=-1)
    turned = jnp.concatenate([-two, one, -four, three], axis=-1)
    return (flat * jnp.cos(angles)[:, None, :] + turned * jnp.sin(angles)[:, None, :]).astype(
        jnp.bfloat16
    )


def fold_block(state, queries, key_block, value_block, scale):
    running, total, accum = state
    scores = (
        jnp.einsum("rkgd,pkd->kgrp", queries, key_block, preferred_element_type=jnp.float32) * scale
    )
    newest = jnp.maximum(running, jnp.max(scores, axis=-1))
    factor = jnp.exp(running - newest)
    expo = jnp.exp(scores - newest[..., None])
    total = total * factor + jnp.sum(expo, axis=-1)
    accum = accum * factor[..., None] + jnp.einsum(
        "kgrp,pkd->kgrd", expo.astype(jnp.bfloat16), value_block, preferred_element_type=jnp.float32
    )
    return (newest, total, accum)


def sweep_keys(state, queries, key_piece, value_piece, scale):
    length = key_piece.shape[0]
    block = math.gcd(length, 2048)
    blocks = length // block
    key_blocks = key_piece.reshape((blocks, block) + key_piece.shape[1:])
    value_blocks = value_piece.reshape((blocks, block) + value_piece.shape[1:])

    def advance(carry, pair):
        return (fold_block(carry, queries, pair[0], pair[1], scale), None)

    state, unused = lax.scan(advance, state, (key_blocks, value_blocks))
    return state


def start_state(queries):
    shape = (queries.shape[1], queries.shape[2], queries.shape[0])
    return (
        jnp.full(shape, -1e30, jnp.float32),
        jnp.zeros(shape, jnp.float32),
        jnp.zeros(shape + (queries.shape[3],), jnp.float32),
    )


def finish(state):
    running, total, accum = state
    outputs = accum / total[..., None]
    count = outputs.shape[2]
    return jnp.transpose(outputs, (2, 0, 1, 3)).reshape(count, -1).astype(jnp.bfloat16)


def local(
    resid,
    query_a,
    key_a,
    value_a,
    query_b,
    key_b,
    value_b,
    gain_qa,
    gain_ka,
    gain_qb,
    gain_kb,
    w_out_a,
    w_out_b,
    norm_gain,
    w_up,
    w_down,
):
    count = query_a.shape[0]
    width_a = gain_qa.shape[0]
    width_b = gain_qb.shape[0]
    places = lax.axis_index("sp") * count + jnp.arange(count, dtype=jnp.int32)
    keys_a = norm_rope(key_a, gain_ka, places)
    keys_b = norm_rope(key_b, gain_kb, places)
    heads_kv_a = keys_a.shape[1]
    heads_kv_b = keys_b.shape[1]
    queries_a = norm_rope(query_a, gain_qa, places)
    queries_b = norm_rope(query_b, gain_qb, places)
    queries_a = queries_a.reshape(count, heads_kv_a, queries_a.shape[1] // heads_kv_a, width_a)
    queries_b = queries_b.reshape(count, heads_kv_b, queries_b.shape[1] // heads_kv_b, width_b)
    values_a = value_a.reshape(count, heads_kv_a, width_a)
    values_b = value_b.reshape(count, heads_kv_b, width_b)
    pieces = side_by_side((keys_a, values_a, keys_b, values_b), "sp", 0, 2)
    state_a = sweep_keys(start_state(queries_a), queries_a, pieces[0], pieces[1], width_a ** (-0.5))
    state_b = sweep_keys(start_state(queries_b), queries_b, pieces[2], pieces[3], width_b ** (-0.5))
    attn_a = finish(state_a)
    attn_b = finish(state_b)
    proj = sum_at_owner(
        (
            jnp.dot(attn_a, w_out_a, preferred_element_type=jnp.float32)
            + jnp.dot(attn_b, w_out_b, preferred_element_type=jnp.float32)
        ).astype(jnp.bfloat16),
        "tp",
        0,
    )
    mid = (resid.astype(jnp.float32) + proj).astype(jnp.bfloat16)
    midf = mid.astype(jnp.float32)
    normed = (
        midf * lax.rsqrt(jnp.mean(midf * midf, axis=-1, keepdims=True) + EPS) * norm_gain
    ).astype(jnp.bfloat16)
    up_whole, down_whole = (
        lax.all_gather(w_up, "sp", axis=0, tiled=True),
        lax.all_gather(w_down, "sp", axis=1, tiled=True),
    )
    hidden = jnp.square(
        jax.nn.relu(
            jnp.dot(gather_directly(normed, "tp", 0), up_whole, preferred_element_type=jnp.float32)
        )
    ).astype(jnp.bfloat16)
    mixed = sum_at_owner(
        jnp.dot(hidden, down_whole, preferred_element_type=jnp.float32).astype(jnp.bfloat16),
        "tp",
        0,
    )
    return (midf + mixed).astype(jnp.bfloat16)


def solution(mesh):
    return jax.shard_map(
        local,
        mesh=mesh,
        in_specs=(
            P(("sp", "tp"), None),
            P("sp", "tp"),
            P("sp", "tp"),
            P("sp", "tp"),
            P("sp", "tp"),
            P("sp", "tp"),
            P("sp", "tp"),
            P(),
            P(),
            P(),
            P(),
            P("tp", None),
            P("tp", None),
            P(),
            P("sp", "tp"),
            P("tp", "sp"),
        ),
        out_specs=P(("sp", "tp"), None),
        check_vma=False,
    )
```

profile of v0, /device:TPU:1, one launch (start us, length us, event | category | flops | bytes accessed | tf_op | source)
XLA Modules:
  0.0 242.3 jit_solution(10272001326339458919)
XLA Ops:
  21.2 46.6 %all-gather.4.cloned.1.call-done = bf16[8192,1,384]{2,0,1:T(8,128)(2,1)} async-done(((bf16[256,1,384]{2,0,1:T(8,128)(2,1)}), bf16[8192,1,384]{2,0,1:T(8,128)(2,1)}) %all-gather.4.cloned.1.call-update) | async-done | bytes 6291472 | tf_op jit(solution)/shard_map/all_gather | solution.py:16
  67.8 3.8 %fusion.91 = (bf16[8192,1,128]{2,0,1:T(8,128)(2,1)S(1)}, bf16[8192,1,128]{2,0,1:T(8,128)(2,1)}) fusion(bf16[8192,1,384]{2,0,1:T(8,128)(2,1)} %all-gather.4.cloned.1.call-done), kind=kLoop, calls=%fused_computation.152 | loop fusion | bytes 8388608 | tf_op jit(solution)/shard_map/slice | solution.py:18
  71.6 36.6 %while.31 = (s32[]{:T(128)}, f32[1,2,256]{2,1,0:T(2,128)S(1)}, f32[1,2,256]{2,1,0:T(2,128)}, f32[1,2,256,128]{3,2,1,0:T(8,128)}, bf16[4,2048,1,128]{3,1,2,0:T(8,...) while((s32[]{:T(128)}, f32[1,2,256]{2,1,0:T(2,128)S(1)}, ...), condition=%wide.region_11.12_spmd.clone, body=%wide.region_8.11_spmd.clone.sunk | while | flops 545459200 | bytes 31113920 | solution.py:97
  71.6 3.8 %bitcast_reduce_fusion.5 = (f32[2,256]{1,0:T(2,128)S(1)}, f32[2048,256,2]{1,0,2:T(8,128)}) fusion(bf16[256,1,2,128]{3,0,2,1:T(8,128)(2,1)} %get-tuple-element.369, bf16[4,2048,1,128]{3,1,2,0:T(8,128)(2,1)} %get-tuple-element.368, s32[]{:T(128)} %get-tuple-element.355), kind=kOutput, calls=%fused_computation.25.clone.1 | convolution fusion | flops 270532096 | bytes 4852224 | tf_op jit(solution)/shard_map/while/body/eval_jaxpr/rkgd,pkd->kgrp/dot_general | solution.py:75
  75.4 3.9 %fusion.120 = f32[1,2,256,128]{3,2,1,0:T(8,128)} fusion(f32[2048,256,2]{1,0,2:T(8,128)} %get-tuple-element.317, f32[2,256]{1,0:T(2,128)S(1)} %bitcast.234, bf16[4,2048,1,128]{3,1,2,0:T(8,128)(2,1)S(1)} %get-tuple-element.370, s32[]{:T(128)} %get-tuple-element.355, f32[1,2,256,128]{3,2,1,0:T(8,128)} %get-tuple-element.358, ...), kind=kOutput, calls=%fused_computation.34.clone.1 | convolution fusion | flops 271777792 | bytes 5246981 | tf_op jit(solution)/shard_map/while/body/eval_jaxpr/kgrp,pkd->kgrd/dot_general | solution.py:81
  84.4 4.0 %fusion.120 = f32[1,2,256,128]{3,2,1,0:T(8,128)} fusion(f32[2048,256,2]{1,0,2:T(8,128)} %get-tuple-element.317, f32[2,256]{1,0:T(2,128)S(1)} %bitcast.234, bf16[4,2048,1,128]{3,1,2,0:T(8,128)(2,1)S(1)} %get-tuple-element.370, s32[]{:T(128)} %get-tuple-element.355, f32[1,2,256,128]{3,2,1,0:T(8,128)} %get-tuple-element.358, ...), kind=kOutput, calls=%fused_computation.34.clone.1 | convolution fusion | flops 271777792 | bytes 5246981 | tf_op jit(solution)/shard_map/while/body/eval_jaxpr/kgrp,pkd->kgrd/dot_general | solution.py:81
  89.7 3.8 %bitcast_reduce_fusion.5 = (f32[2,256]{1,0:T(2,128)S(1)}, f32[2048,256,2]{1,0,2:T(8,128)}) fusion(bf16[256,1,2,128]{3,0,2,1:T(8,128)(2,1)} %get-tuple-element.369, bf16[4,2048,1,128]{3,1,2,0:T(8,128)(2,1)} %get-tuple-element.368, s32[]{:T(128)} %get-tuple-element.355), kind=kOutput, calls=%fused_computation.25.clone.1 | convolution fusion | flops 270532096 | bytes 4852224 | tf_op jit(solution)/shard_map/while/body/eval_jaxpr/rkgd,pkd->kgrp/dot_general | solution.py:75
  93.5 3.9 %fusion.120 = f32[1,2,256,128]{3,2,1,0:T(8,128)} fusion(f32[2048,256,2]{1,0,2:T(8,128)} %get-tuple-element.317, f32[2,256]{1,0:T(2,128)S(1)} %bitcast.234, bf16[4,2048,1,128]{3,1,2,0:T(8,128)(2,1)S(1)} %get-tuple-element.370, s32[]{:T(128)} %get-tuple-element.355, f32[1,2,256,128]{3,2,1,0:T(8,128)} %get-tuple-element.358, ...), kind=kOutput, calls=%fused_computation.34.clone.1 | convolution fusion | flops 271777792 | bytes 5246981 | tf_op jit(solution)/shard_map/while/body/eval_jaxpr/kgrp,pkd->kgrd/dot_general | solution.py:81
  98.8 4.0 %bitcast_reduce_fusion.5 = (f32[2,256]{1,0:T(2,128)S(1)}, f32[2048,256,2]{1,0,2:T(8,128)}) fusion(bf16[256,1,2,128]{3,0,2,1:T(8,128)(2,1)} %get-tuple-element.369, bf16[4,2048,1,128]{3,1,2,0:T(8,128)(2,1)} %get-tuple-element.368, s32[]{:T(128)} %get-tuple-element.355), kind=kOutput, calls=%fused_computation.25.clone.1 | convolution fusion | flops 270532096 | bytes 4852224 | tf_op jit(solution)/shard_map/while/body/eval_jaxpr/rkgd,pkd->kgrp/dot_general | solution.py:75
  102.8 4.1 %fusion.120 = f32[1,2,256,128]{3,2,1,0:T(8,128)} fusion(f32[2048,256,2]{1,0,2:T(8,128)} %get-tuple-element.317, f32[2,256]{1,0:T(2,128)S(1)} %bitcast.234, bf16[4,2048,1,128]{3,1,2,0:T(8,128)(2,1)S(1)} %get-tuple-element.370, s32[]{:T(128)} %get-tuple-element.355, f32[1,2,256,128]{3,2,1,0:T(8,128)} %get-tuple-element.358, ...), kind=kOutput, calls=%fused_computation.34.clone.1 | convolution fusion | flops 271777792 | bytes 5246981 | tf_op jit(solution)/shard_map/while/body/eval_jaxpr/kgrp,pkd->kgrd/dot_general | solution.py:81
  109.9 4.5 %fusion.92 = (bf16[8192,1,64]{2,0,1:T(8,128)(2,1)S(1)}, bf16[8192,1,64]{2,0,1:T(8,128)(2,1)}) fusion(bf16[8192,1,384]{2,0,1:T(8,128)(2,1)} %all-gather.4.cloned.1.call-done), kind=kLoop, calls=%fused_computation.153 | loop fusion | bytes 4194304 | tf_op jit(solution)/shard_map/slice | solution.py:18
  119.7 52.6 %while.30 = (s32[]{:T(128)}, f32[1,4,256]{2,1,0:T(4,128)S(1)}, f32[1,4,256]{2,1,0:T(4,128)S(1)}, f32[1,4,256,64]{2,3,1,0:T(8,128)S(1)}, bf16[4,2048,1,64]{1,3,2,...) while((s32[]{:T(128)}, f32[1,4,256]{2,1,0:T(4,128)S(1)}, ...), condition=%wide.region_6.7_spmd.clone, body=%wide.region_3.6_spmd.clone.sunk | while | flops 553850880 | bytes 59966592 | solution.py:97
  119.8 5.5 %bitcast_reduce_fusion.4 = (f32[4,256]{1,0:T(4,128)S(1)}, f32[2048,256,4]{1,0,2:T(8,128)}) fusion(bf16[256,1,4,64]{0,3,2,1:T(8,128)(2,1)S(1)} %get-tuple-element.342, bf16[4,2048,1,64]{1,3,2,0:T(8,128)(2,1)} %get-tuple-element.341, s32[]{:T(128)} %get-tuple-element.328), kind=kOutput, calls=%fused_computation.1.clone.1 | convolution fusion | flops 272628736 | bytes 8786432 | tf_op jit(solution)/shard_map/while/body/eval_jaxpr/rkgd,pkd->kgrp/dot_general | solution.py:75
  125.3 5.2 %fusion.115 = f32[1,4,256,64]{2,3,1,0:T(8,128)S(1)} fusion(f32[2048,256,4]{1,0,2:T(8,128)} %get-tuple-element.306, f32[4,256]{1,0:T(4,128)S(1)} %bitcast.231, f32[1,4,256,64]{2,3,1,0:T(8,128)S(1)} %get-tuple-element.331, bf16[4,2048,1,64]{1,3,2,0:T(8,128)(2,1)} %get-tuple-element.343, s32[]{:T(128)} %get-tuple-element.328, ...), kind=kOutput, calls=%fused_computation.8.clone.1 | convolution fusion | flops 274923520 | bytes 9183745 | tf_op jit(solution)/shard_map/while/body/eval_jaxpr/kgrp,pkd->kgrd/dot_general | solution.py:81
  132.5 5.5 %bitcast_reduce_fusion.4 = (f32[4,256]{1,0:T(4,128)S(1)}, f32[2048,256,4]{1,0,2:T(8,128)}) fusion(bf16[256,1,4,64]{0,3,2,1:T(8,128)(2,1)S(1)} %get-tuple-element.342, bf16[4,2048,1,64]{1,3,2,0:T(8,128)(2,1)} %get-tuple-element.341, s32[]{:T(128)} %get-tuple-element.328), kind=kOutput, calls=%fused_computation.1.clone.1 | convolution fusion | flops 272628736 | bytes 8786432 | tf_op jit(solution)/shard_map/while/body/eval_jaxpr/rkgd,pkd->kgrp/dot_general | solution.py:75
  138.0 5.2 %fusion.115 = f32[1,4,256,64]{2,3,1,0:T(8,128)S(1)} fusion(f32[2048,256,4]{1,0,2:T(8,128)} %get-tuple-element.306, f32[4,256]{1,0:T(4,128)S(1)} %bitcast.231, f32[1,4,256,64]{2,3,1,0:T(8,128)S(1)} %get-tuple-element.331, bf16[4,2048,1,64]{1,3,2,0:T(8,128)(2,1)} %get-tuple-element.343, s32[]{:T(128)} %get-tuple-element.328, ...), kind=kOutput, calls=%fused_computation.8.clone.1 | convolution fusion | flops 274923520 | bytes 9183745 | tf_op jit(solution)/shard_map/while/body/eval_jaxpr/kgrp,pkd->kgrd/dot_general | solution.py:81
  145.4 5.5 %bitcast_reduce_fusion.4 = (f32[4,256]{1,0:T(4,128)S(1)}, f32[2048,256,4]{1,0,2:T(8,128)}) fusion(bf16[256,1,4,64]{0,3,2,1:T(8,128)(2,1)S(1)} %get-tuple-element.342, bf16[4,2048,1,64]{1,3,2,0:T(8,128)(2,1)} %get-tuple-element.341, s32[]{:T(128)} %get-tuple-element.328), kind=kOutput, calls=%fused_computation.1.clone.1 | convolution fusion | flops 272628736 | bytes 8786432 | tf_op jit(solution)/shard_map/while/body/eval_jaxpr/rkgd,pkd->kgrp/dot_general | solution.py:75
  150.9 5.4 %fusion.115 = f32[1,4,256,64]{2,3,1,0:T(8,128)S(1)} fusion(f32[2048,256,4]{1,0,2:T(8,128)} %get-tuple-element.306, f32[4,256]{1,0:T(4,128)S(1)} %bitcast.231, f32[1,4,256,64]{2,3,1,0:T(8,128)S(1)} %get-tuple-element.331, bf16[4,2048,1,64]{1,3,2,0:T(8,128)(2,1)} %get-tuple-element.343, s32[]{:T(128)} %get-tuple-element.328, ...), kind=kOutput, calls=%fused_computation.8.clone.1 | convolution fusion | flops 274923520 | bytes 9183745 | tf_op jit(solution)/shard_map/while/body/eval_jaxpr/kgrp,pkd->kgrd/dot_general | solution.py:81
  158.8 5.5 %bitcast_reduce_fusion.4 = (f32[4,256]{1,0:T(4,128)S(1)}, f32[2048,256,4]{1,0,2:T(8,128)}) fusion(bf16[256,1,4,64]{0,3,2,1:T(8,128)(2,1)S(1)} %get-tuple-element.342, bf16[4,2048,1,64]{1,3,2,0:T(8,128)(2,1)} %get-tuple-element.341, s32[]{:T(128)} %get-tuple-element.328), kind=kOutput, calls=%fused_computation.1.clone.1 | convolution fusion | flops 272628736 | bytes 8786432 | tf_op jit(solution)/shard_map/while/body/eval_jaxpr/rkgd,pkd->kgrp/dot_general | solution.py:75
  164.4 5.5 %fusion.115 = f32[1,4,256,64]{2,3,1,0:T(8,128)S(1)} fusion(f32[2048,256,4]{1,0,2:T(8,128)} %get-tuple-element.306, f32[4,256]{1,0:T(4,128)S(1)} %bitcast.231, f32[1,4,256,64]{2,3,1,0:T(8,128)S(1)} %get-tuple-element.331, bf16[4,2048,1,64]{1,3,2,0:T(8,128)(2,1)} %get-tuple-element.343, s32[]{:T(128)} %get-tuple-element.328, ...), kind=kOutput, calls=%fused_computation.8.clone.1 | convolution fusion | flops 274923520 | bytes 9183745 | tf_op jit(solution)/shard_map/while/body/eval_jaxpr/kgrp,pkd->kgrd/dot_general | solution.py:81
  174.0 18.3 %all_to_all.15 = bf16[4,64,2048]{2,1,0:T(8,128)(2,1)S(1)} all-to-all(bf16[4,64,2048]{2,1,0:T(8,128)(2,1)S(1)} %bitcast.230), channel_id=1, replica_groups=mesh['sp'=32,'tp'=4] {'tp'}, dimensions={0} | all-to-all | bytes 2097152 | tf_op jit(solution)/shard_map/all_to_all | solution.py:31
  193.0 16.4 %all_to_all.16 = bf16[4,64,2048]{2,1,0:T(8,128)(2,1)S(1)} all-to-all(bf16[4,64,2048]{2,1,0:T(8,128)(2,1)S(1)} %broadcast_in_dim.20), channel_id=1, replica_groups=mesh['sp'=32,'tp'=4] {'tp'}, dimensions={0} | all-to-all | bytes 2097152 | tf_op jit(solution)/shard_map/all_to_all | solution.py:37
  209.4 10.3 %convolution_convert_fusion = bf16[256,2048]{1,0:T(8,128)(2,1)S(1)} fusion(bf16[2048,2048]{0,1:T(8,128)(2,1)} %all-gather.8.cloned.1.call-done, bf16[256,2048]{1,0:T(8,128)(2,1)S(1)} %bitcast.236, bf16[2048,2048]{1,0:T(8,128)(2,1)} %all-gather.6.cloned.1.call-done), kind=kOutput, calls=%fused_computation.56 | convolution fusion | flops 4297064448 | bytes 18874368 | tf_op jit(solution)/shard_map/dot_general | solution.py:177
  219.7 15.2 %all_to_all.17 = bf16[4,64,2048]{2,1,0:T(8,128)(2,1)S(1)} all-to-all(bf16[4,64,2048]{2,1,0:T(8,128)(2,1)S(1)} %bitcast.237), channel_id=1, replica_groups=mesh['sp'=32,'tp'=4] {'tp'}, dimensions={0} | all-to-all | bytes 2097152 | tf_op jit(solution)/shard_map/all_to_all | solution.py:31
  (146 shorter events, 42.8 us)
Async XLA Ops:
  6.5 165.9 %copy-start = (bf16[256,2048]{1,0:T(8,128)(2,1)S(1)}, bf16[256,2048]{1,0:T(8,128)(2,1)}, u32[]{:S(2)}) copy-start(bf16[256,2048]{1,0:T(8,128)(2,1)} %param.31) | copy-start | bytes 3145732
  6.5 6.9 %copy-start.11 = (f32[64]{0:T(128)S(1)}, f32[64]{0:T(128)}, u32[]{:S(2)}) copy-start(f32[64]{0:T(128)} %param.28) | copy-start | bytes 772
  6.5 7.5 %copy-start.9 = (bf16[256,128]{1,0:T(8,128)(2,1)S(1)}, bf16[256,128]{1,0:T(8,128)(2,1)}, u32[]{:S(2)}) copy-start(bf16[256,128]{1,0:T(8,128)(2,1)} %param.26) | copy-start | bytes 196612
  6.5 61.2 %all-gather.4.cloned.1.call-start = ((), (), s32[]{:S(2)}) async-start(), calls=%async_computation.3 | async-start | bytes 6488064 | tf_op jit(solution)/shard_map/all_gather | solution.py:16
  10.5 9.6 %copy-start.5 = (bf16[256,256]{1,0:T(8,128)(2,1)S(1)}, bf16[256,256]{1,0:T(8,128)(2,1)}, u32[]{:S(2)}) copy-start(bf16[256,256]{1,0:T(8,128)(2,1)} %param.21) | copy-start | bytes 393220
  13.4 7.7 %copy-start.12 = (f32[64]{0:T(128)S(1)}, f32[64]{0:T(128)}, u32[]{:S(2)}) copy-start(f32[64]{0:T(128)} %param.27) | copy-start | bytes 772
  14.9 194.5 %all-gather.6.cloned.1.call-start = ((), (), s32[]{:S(2)}) async-start(), calls=%async_computation.4 | async-start | bytes 8650752 | tf_op jit(solution)/shard_map/all_gather | solution.py:168
  15.6 193.8 %all-gather.8.cloned.1.call-start = ((), (), s32[]{:S(2)}) async-start(), calls=%async_computation.5 | async-start | bytes 8650752 | tf_op jit(solution)/shard_map/all_gather | solution.py:169
  75.4 4.0 %copy-start.2 = (f32[2048,256,2]{1,0,2:T(8,128)S(1)}, f32[2048,256,2]{1,0,2:T(8,128)}, u32[]{:S(2)}) copy-start(f32[2048,256,2]{1,0,2:T(8,128)} %get-tuple-element.317) | copy-start | bytes 12582916 | tf_op jit(solution)/shard_map/while
  75.4 4.6 %copy-start.6 = (f32[1,2,256]{2,1,0:T(2,128)S(1)}, f32[1,2,256]{2,1,0:T(2,128)}, u32[]{:S(2)}) copy-start(f32[1,2,256]{2,1,0:T(2,128)} %get-tuple-element.357) | copy-start | bytes 6148 | tf_op jit(solution)/shard_map/while
  84.4 4.0 %copy-start.2 = (f32[2048,256,2]{1,0,2:T(8,128)S(1)}, f32[2048,256,2]{1,0,2:T(8,128)}, u32[]{:S(2)}) copy-start(f32[2048,256,2]{1,0,2:T(8,128)} %get-tuple-element.317) | copy-start | bytes 12582916 | tf_op jit(solution)/shard_map/while
  84.4 4.7 %copy-start.6 = (f32[1,2,256]{2,1,0:T(2,128)S(1)}, f32[1,2,256]{2,1,0:T(2,128)}, u32[]{:S(2)}) copy-start(f32[1,2,256]{2,1,0:T(2,128)} %get-tuple-element.357) | copy-start | bytes 6148 | tf_op jit(solution)/shard_map/while
  93.5 4.0 %copy-start.2 = (f32[2048,256,2]{1,0,2:T(8,128)S(1)}, f32[2048,256,2]{1,0,2:T(8,128)}, u32[]{:S(2)}) copy-start(f32[2048,256,2]{1,0,2:T(8,128)} %get-tuple-element.317) | copy-start | bytes 12582916 | tf_op jit(solution)/shard_map/while
  93.5 4.7 %copy-start.6 = (f32[1,2,256]{2,1,0:T(2,128)S(1)}, f32[1,2,256]{2,1,0:T(2,128)}, u32[]{:S(2)}) copy-start(f32[1,2,256]{2,1,0:T(2,128)} %get-tuple-element.357) | copy-start | bytes 6148 | tf_op jit(solution)/shard_map/while
  102.8 4.1 %copy-start.2 = (f32[2048,256,2]{1,0,2:T(8,128)S(1)}, f32[2048,256,2]{1,0,2:T(8,128)}, u32[]{:S(2)}) copy-start(f32[2048,256,2]{1,0,2:T(8,128)} %get-tuple-element.317) | copy-start | bytes 12582916 | tf_op jit(solution)/shard_map/while
  102.8 4.8 %copy-start.6 = (f32[1,2,256]{2,1,0:T(2,128)S(1)}, f32[1,2,256]{2,1,0:T(2,128)}, u32[]{:S(2)}) copy-start(f32[1,2,256]{2,1,0:T(2,128)} %get-tuple-element.357) | copy-start | bytes 6148 | tf_op jit(solution)/shard_map/while
  114.4 4.4 %copy-start.8 = (f32[1,2,256]{2,1,0:T(2,128)S(1)}, f32[1,2,256]{2,1,0:T(2,128)}, u32[]{:S(2)}) copy-start(f32[1,2,256]{2,1,0:T(2,128)} %get-tuple-element.84) | copy-start | bytes 6148
  125.2 5.9 %copy-start.1 = (f32[2048,256,4]{1,0,2:T(8,128)S(1)}, f32[2048,256,4]{1,0,2:T(8,128)}, u32[]{:S(2)}) copy-start(f32[2048,256,4]{1,0,2:T(8,128)} %get-tuple-element.306) | copy-start | bytes 25165828 | tf_op jit(solution)/shard_map/while
  138.0 6.0 %copy-start.1 = (f32[2048,256,4]{1,0,2:T(8,128)S(1)}, f32[2048,256,4]{1,0,2:T(8,128)}, u32[]{:S(2)}) copy-start(f32[2048,256,4]{1,0,2:T(8,128)} %get-tuple-element.306) | copy-start | bytes 25165828 | tf_op jit(solution)/shard_map/while
  150.9 6.5 %copy-start.1 = (f32[2048,256,4]{1,0,2:T(8,128)S(1)}, f32[2048,256,4]{1,0,2:T(8,128)}, u32[]{:S(2)}) copy-start(f32[2048,256,4]{1,0,2:T(8,128)} %get-tuple-element.306) | copy-start | bytes 25165828 | tf_op jit(solution)/shard_map/while
  164.4 6.5 %copy-start.1 = (f32[2048,256,4]{1,0,2:T(8,128)S(1)}, f32[2048,256,4]{1,0,2:T(8,128)}, u32[]{:S(2)}) copy-start(f32[2048,256,4]{1,0,2:T(8,128)} %get-tuple-element.306) | copy-start | bytes 25165828 | tf_op jit(solution)/shard_map/while
  172.3 1.2 copy-start.3
  172.9 19.7 %copy-start.4 = (bf16[64,2048]{1,0:T(8,128)(2,1)S(1)}, bf16[64,2048]{1,0:T(8,128)(2,1)}, u32[]{:S(2)}) copy-start(bf16[64,2048]{1,0:T(8,128)(2,1)} %param.20) | copy-start | bytes 786436
  173.6 19.2 %copy-start.10 = (f32[2048]{0:T(1024)S(1)}, f32[2048]{0:T(1024)}, u32[]{:S(2)}) copy-start(f32[2048]{0:T(1024)} %param.33) | copy-start | bytes 24580
  (4 other events, 2.3 us)
Sparse Core Ops, SparseCore 0:
  15.0 52.7 all-gather.3
  70.0 51.5 all-gather.5
  123.9 52.3 all-gather.7
where the time goes:
time: 245 us; the launch traced here: 242 us
  matrix products  85.7 us (35%)
  blocking collectives  49.9 us (20%)
  waiting for transfers between devices  47.8 us (20%)
  local copies, waits for them, and re-layouts  25.1 us (10%)
  other arithmetic  19.8 us (8%)
  between operations  13.5 us (6%)
    all_gather x1, waiting for transfers between devices, side_by_side(): result, at, outs = (lax.all_gather(both, axis, axis=dim, tiled=True), 0, [])  46.6 us
    dot_general x8, matrix products, fold_block(): jnp.einsum('rkgd,pkd->kgrp', queries, key_block, preferred_element_type=j...  37.3 us
    dot_general x8, matrix products, fold_block(): jnp.einsum('kgrp,pkd->kgrd', expo.astype(jnp.bfloat16), value_block, pref...  37.2 us
    all_to_all x2, blocking collectives, sum_at_owner(): lax.all_to_all(split_up(shard, dim, length), axis, 0, 0, tiled=True)  33.6 us
    all_to_all x1, blocking collectives, copy_for_each(): lax.all_to_all(jnp.broadcast_to(shard[None], (length, *shard.shape)), axi...  16.4 us
    dot_general x1, matrix products, local(): jnp.dot(hidden, down_whole, preferred_element_type=jnp.float32)  10.3 us
    unnamed x24, local copies, waits for them, and re-layouts  8.59 us
    slice x2, local copies, waits for them, and re-layouts, side_by_side(): outs.append(lax.slice_in_dim(result, at, at + a.shape[along], axis=along))  8.29 us
  transfers between devices with their start and end apart: 3, of which 1 were waited for; matrix products, arithmetic and copies ran while one was open for 43% of the time, Pallas kernels for 0%

commit v1 on v0

v1 whole, which is shorter than its diff:
```python
import functools
import math

import jax
import jax.numpy as jnp
import numpy as np
from jax import lax
from jax.experimental import pallas as pl
from jax.experimental.pallas import tpu as pltpu
from jax.sharding import PartitionSpec as P

MESH = pl.DeviceIdType.MESH
EPS = 1e-06
F32 = jnp.float32
BF16 = jnp.bfloat16
LOG2E = 1.4426950408889634
KV, UP, DOWN = 0, 1, 2
PLACES = (0, 3, 1, 2)


def build_tables():
    rows, cols = [], []
    for width in (64, 128):
        quarter = width // 4
        freqs = (10000.0 ** (-(2.0 * np.arange(quarter)) / (width // 2))).astype(np.float32)
        freqs = np.concatenate([freqs, freqs])
        entry = np.arange(width)
        sign = np.where((entry // quarter) % 2 == 0, -1.0, 1.0)

        def pair(count, low):
            ang = (np.arange(count, dtype=np.float32)[:, None] * freqs).astype(np.float64)
            full = np.zeros((2, count, width))
            half = slice(0, width // 2) if low else slice(width // 2, width)
            full[0][:, half] = np.cos(ang)
            full[1][:, half] = np.sin(ang)
            full[1] *= sign
            return np.tile(full, (1, 1, 128 // width)).astype(np.float32)

        rows.append(pair(128, True))
        cols.append(pair(64, False))
    row = np.concatenate(rows, axis=0)
    row = row.reshape(4, 32, 4, 128).transpose(1, 0, 2, 3).reshape(32, 16, 128)
    col = np.concatenate(cols, axis=0)
    return row, col


def nt_dot(a, b):
    return lax.dot_general(a, b, (((1,), (1,)), ((), ())), preferred_element_type=F32)


def place(k):
    return (3 * k + 3 * (k // 2) + 2 * (k // 3)) % 4


def plan():
    def wave(item):
        return [
            (item, 3, 0), (item, 1, 0), (item, 0, 3), (item, 0, 1), (item, 2, 0), (item, 0, 2),
            (item, 3, 3), (item, 3, 1), (item, 1, 3), (item, 1, 1), (item, 3, 2), (item, 1, 2),
            (item, 2, 3), (item, 2, 1), (item, 2, 2),
        ]

    k, u, d = wave(KV), wave(UP), wave(DOWN)
    steps = [[] for _ in range(16)]
    steps[1] = k[0:4]
    steps[2] = u[0:2]
    steps[3] = k[4:6]
    steps[4] = u[2:4]
    steps[5] = k[6:8]
    steps[6] = u[4:5]
    steps[7] = k[8:11]
    steps[8] = u[5:7]
    steps[9] = [k[11]]
    steps[10] = u[7:8]
    steps[11] = [k[12]]
    steps[12] = [k[13]] + u[8:9]
    steps[13] = [k[14]]
    steps[14] = u[9:11]
    steps[15] = [(DOWN, 0, 0)]
    return steps, u[11:], d


def kernel(
    qa_ref, ka_ref, va_ref, qb_ref, kb_ref, vb_ref, gains_ref, ngain_ref, rowtab_ref, coltab_ref,
    resid_hbm, woa_hbm, wob_hbm, wup_hbm, wdown_hbm,
    out_ref,
    kvbuf, wbuf, wd_in, wo, resid, qa, qb, m_a, m_b, acc_a, acc_b, attn,
    pout, rsbuf, nbuf, hidden, dbuf, frecv, stage, midbuf,
    lsem, ssem, rsem, psend, precv, xs, xr, fs, fr,
):
    sp = lax.axis_index("sp")
    x = lax.axis_index("tp")
    z, y, c = sp // 8, (sp // 2) % 4, sp % 2
    n = 1 - c
    partner = z * 8 + y * 2 + n

    def slot(da, db):
        return ((z + n * db + c * da) % 4) * 8 + ((y + n * da + c * db) % 4) * 2 + c

    def partner_slot(da, db):
        return ((z + c * db + n * da) % 4) * 8 + ((y + c * da + n * db) % 4) * 2 + n

    def event(da, db):
        return PLACES.index(da) * 4 + PLACES.index(db)

    barrier = pltpu.get_barrier_semaphore()
    others = [(slot(1, 0), x), (slot(3, 0), x), (slot(0, 1), x), (slot(0, 3), x), (partner, x)]
    others += [(sp, (x + d) % 4) for d in (1, 2, 3)]
    for dev in others:
        pl.semaphore_signal(barrier, inc=1, device_id=dev, device_id_type=MESH)

    loads = [
        pltpu.make_async_copy(wup_hbm, wbuf.at[0, sp], lsem.at[0]),
        pltpu.make_async_copy(wdown_hbm, wd_in, lsem.at[1]),
        pltpu.make_async_copy(woa_hbm, wo.at[pl.ds(0, 256)], lsem.at[2]),
        pltpu.make_async_copy(wob_hbm, wo.at[pl.ds(256, 256)], lsem.at[3]),
        pltpu.make_async_copy(resid_hbm, resid, lsem.at[4]),
    ]
    for load in loads:
        load.start()

    def region(item, index, half):
        if item == KV:
            ref, size = kvbuf.at[index], 128
        else:
            ref, size = wbuf.at[item - 1, index], 32
        if half is None:
            return ref
        return ref.at[pl.ds(half * size, size)]

    sends = []

    def send(item, ev, number, index, half, to, there):
        piece = region(item, index, half)
        copy = pltpu.make_async_remote_copy(
            src_ref=piece,
            dst_ref=piece,
            send_sem=ssem.at[item, ev, number],
            recv_sem=rsem.at[item, event(*there), 0 if half is None else half],
            device_id=(slot(*to), x),
            device_id_type=MESH,
        )
        copy.start()
        sends.append((item, ev, number, half))

    def hand_over(item, ev, index):
        piece = region(item, index, None)
        pltpu.make_async_remote_copy(
            src_ref=piece,
            dst_ref=piece,
            send_sem=psend.at[item, ev],
            recv_sem=precv.at[item, ev],
            device_id=(partner, x),
            device_id_type=MESH,
        ).start()

    def wait_in(item, ev, index, half):
        piece = region(item, index, half)
        pltpu.make_async_remote_copy(
            src_ref=piece,
            dst_ref=piece,
            send_sem=ssem.at[item, ev, 0],
            recv_sem=rsem.at[item, ev, 0 if half is None else half],
            device_id=(partner, x),
            device_id_type=MESH,
        ).wait_recv()

    def wait_partner(item, ev, index):
        piece = region(item, index, None)
        pltpu.make_async_remote_copy(
            src_ref=piece,
            dst_ref=piece,
            send_sem=psend.at[item, ev],
            recv_sem=precv.at[item, ev],
            device_id=(partner, x),
            device_id_type=MESH,
        ).wait_recv()

    def take(item, da, db):
        ev, index = event(da, db), slot(da, db)
        if da == 0 and db == 0:
            send(item, ev, 0, index, None, (1, 0), (3, 0))
            send(item, ev, 1, index, None, (3, 0), (1, 0))
            send(item, ev, 2, index, None, (0, 1), (0, 3))
            send(item, ev, 3, index, None, (0, 3), (0, 1))
        elif db == 0:
            if da == 2:
                wait_in(item, ev, index, 0)
                wait_in(item, ev, index, 1)
            else:
                wait_in(item, ev, index, None)
                if da == 3:
                    send(item, ev, 0, index, 0, (1, 0), (2, 0))
                else:
                    send(item, ev, 0, index, 1, (3, 0), (2, 0))
            send(item, ev, 2, index, None, (0, 1), (da, 3))
            send(item, ev, 3, index, None, (0, 3), (da, 1))
        elif db == 2:
            wait_in(item, ev, index, 0)
            wait_in(item, ev, index, 1)
        else:
            wait_in(item, ev, index, None)
            if db == 3:
                send(item, ev, 0, index, 0, (0, 1), (da, 2))
            else:
                send(item, ev, 0, index, 1, (0, 3), (da, 2))
        hand_over(item, ev, index)

    lane = lax.broadcasted_iota(jnp.int32, (64, 128), 1)
    low = lane < 64
    rowtab = rowtab_ref[sp]

    def rotate(v, gain, width, r):
        quarter = width // 4
        kind = 0 if width == 64 else 2
        cosine = rowtab[kind * 4 + r][None, :] + coltab_ref[kind]
        sine = rowtab[(kind + 1) * 4 + r][None, :] + coltab_ref[kind + 1]
        sq = v * v
        if width == 64:
            left = jnp.sum(jnp.where(low, sq, 0.0), axis=-1, keepdims=True)
            right = jnp.sum(jnp.where(low, 0.0, sq), axis=-1, keepdims=True)
            mean = jnp.where(low, left, right) * (1.0 / 64)
        else:
            mean = jnp.sum(sq, axis=-1, keepdims=True) * (1.0 / 128)
        u = v * lax.rsqrt(mean + EPS) * gain
        even = (lane // quarter) % 2 == 0
        turned = jnp.where(even, pltpu.roll(u, 128 - quarter, 1), pltpu.roll(u, quarter, 1))
        return u * cosine + turned * sine

    own = slot(0, 0)
    for r in range(4):
        rows = pl.ds(r * 64, 64)
        both = jnp.concatenate([ka_ref[rows, :].astype(F32), va_ref[rows, :].astype(F32)], axis=1)
        turned = rotate(both, gains_ref[1:2, :], 64, r)
        kvbuf[own, rows, 0:128] = jnp.where(low, turned, both).astype(BF16)
        kvbuf[own, rows, 128:256] = rotate(kb_ref[rows, :].astype(F32), gains_ref[3:4, :], 128, r).astype(BF16)
        kvbuf[own, rows, 256:384] = vb_ref[rows, :]

    pl.semaphore_wait(barrier, len(others))
    take(KV, 0, 0)

    for r in range(4):
        rows = pl.ds(r * 64, 64)
        for g in range(2):
            v = rotate(qa_ref[rows, g * 128 : (g + 1) * 128].astype(F32), gains_ref[0:1, :], 64, r)
            qa[pl.ds((2 * g) * 256 + r * 64, 64), :] = jnp.where(low, v, 0.0).astype(BF16)
            qa[pl.ds((2 * g + 1) * 256 + r * 64, 64), :] = jnp.where(low, pltpu.roll(v, 64, 1), 0.0).astype(BF16)
            w = rotate(qb_ref[rows, g * 128 : (g + 1) * 128].astype(F32), gains_ref[2:3, :], 128, r)
            qb[pl.ds(g * 256 + r * 64, 64), :] = w.astype(BF16)

    loads[0].wait()
    take(UP, 0, 0)

    m_a[...] = jnp.full_like(m_a, -1e30)
    m_b[...] = jnp.full_like(m_b, -1e30)
    acc_a[...] = jnp.zeros_like(acc_a)
    acc_b[...] = jnp.zeros_like(acc_b)

    loads[1].wait()
    for g in range(4):
        block = wd_in[pl.ds(g * 512, 512), :].astype(F32)
        wbuf[1, own, :, g * 512 : (g + 1) * 512] = block.T.astype(BF16)

    steps, rest_up, rest_down = plan()
    lane512 = lax.broadcasted_iota(jnp.int32, (512, 128), 1)
    scale_a = 64 ** (-0.5) * LOG2E
    scale_b = 128 ** (-0.5) * LOG2E

    def fold(queries, keys, values, m_ref, acc_ref, start, scale):
        rows = pl.ds(start, 256)
        scores = nt_dot(queries[rows, :], keys) * scale
        before = m_ref[rows, :]
        top = jnp.maximum(before, jnp.max(scores, axis=-1, keepdims=True))
        m_ref[rows, :] = top
        factor = jnp.exp2(before - top)
        expo = jnp.exp2(scores - top[:, 0:1]).astype(BF16)
        got = jnp.dot(expo, values, preferred_element_type=F32)
        if acc_ref.shape[1] == 256:
            factor = jnp.concatenate([factor, factor], axis=1)
        acc_ref[rows, :] = acc_ref[rows, :] * factor + got

    def attend(i, carry):
        for number, events in enumerate(steps):
            if events:

                @pl.when(i == number)
                def _(events=events):
                    for item, da, db in events:
                        take(item, da, db)

        da, db = place(i // 4), place(i % 4)
        mine, other = slot(da, db), partner_slot(da, db)
        wait_partner(KV, i, other)
        keys = jnp.concatenate([kvbuf[mine, :, 0:128], kvbuf[other, :, 0:128]], axis=0)
        values = jnp.where(lane512 < 64, jnp.ones_like(keys), keys)
        for h in range(4):
            fold(qa, keys, values, m_a, acc_a, h * 256, scale_a)
        keys = jnp.concatenate([kvbuf[mine, :, 128:256], kvbuf[other, :, 128:256]], axis=0)
        values = jnp.concatenate([kvbuf[mine, :, 256:384], kvbuf[other, :, 256:384]], axis=0)
        values = jnp.concatenate([values, jnp.ones_like(values)], axis=1)
        for h in range(2):
            fold(qb, keys, values, m_b, acc_b, h * 256, scale_b)
        return carry

    lax.fori_loop(0, 16, attend, 0)

    low256 = lax.broadcasted_iota(jnp.int32, (256, 128), 1) < 64
    for g in range(2):
        halves = []
        for h in (2 * g, 2 * g + 1):
            acc = acc_a[h * 256 : (h + 1) * 256, :]
            halves.append(acc / acc[:, 0:1])
        both = jnp.where(low256, pltpu.roll(halves[0], 64, 1), halves[1])
        attn[:, g * 128 : (g + 1) * 128] = both.astype(BF16)
        acc = acc_b[g * 256 : (g + 1) * 256, :]
        attn[:, 256 + g * 128 : 256 + (g + 1) * 128] = (acc[:, 0:128] / acc[:, 128:256]).astype(BF16)
    loads[2].wait()
    loads[3].wait()

    def project(j, carry):
        cols = pl.ds(pl.multiple_of(j * 512, 512), 512)
        part = jnp.dot(attn[...], wo[:, cols], preferred_element_type=F32).astype(BF16)
        for r in range(4):
            pout[r, :, cols] = part[r * 64 : (r + 1) * 64, :]
        return carry

    lax.fori_loop(0, 4, project, 0)

    def to_peer(d, src, dst, ssems, rsems):
        return pltpu.make_async_remote_copy(
            src_ref=src,
            dst_ref=dst,
            send_sem=ssems,
            recv_sem=rsems,
            device_id=(sp, (x + d) % 4),
            device_id_type=MESH,
        )

    def rs_copy(d):
        return to_peer(d, pout.at[(x + d) % 4], rsbuf.at[d - 1], xs.at[0, d - 1], xr.at[0, d - 1])

    for d in (2, 1, 3):
        rs_copy(d).start()
    for item, da, db in rest_up:
        take(item, da, db)
    for item, da, db in rest_down[0:2]:
        take(item, da, db)
    loads[4].wait()
    for d in (1, 3, 2):
        rs_copy(d).wait_recv()
    total = pout[x].astype(F32)
    for d in range(3):
        total = total + rsbuf[d].astype(F32)
    mid = (resid[...].astype(F32) + total).astype(BF16).astype(F32)
    midbuf[...] = mid
    norm = mid * lax.rsqrt(jnp.mean(mid * mid, axis=-1, keepdims=True) + EPS) * ngain_ref[...]
    nbuf[x] = norm.astype(BF16)

    def ag_copy(d, there):
        index = (x + d) % 4 if there else x
        return to_peer(d, nbuf.at[index], nbuf.at[index], xs.at[1, d - 1], xr.at[1, d - 1])

    for d in (2, 1, 3):
        ag_copy(d, False).start()
    for item, da, db in rest_down[2:6]:
        take(item, da, db)
    for ev in range(16):
        wait_partner(UP, ev, partner_slot(PLACES[ev // 4], PLACES[ev % 4]))
    for d in (1, 3, 2):
        to_peer(d, nbuf.at[(x + 4 - d) % 4], nbuf.at[(x + 4 - d) % 4], xs.at[1, d - 1], xr.at[1, d - 1]).wait_recv()

    def up(j, carry):
        cols = pl.ds(pl.multiple_of(j * 256, 256), 256)
        rows = nbuf[...].reshape(256, 2048)
        weights = wbuf[0, :, :, cols].reshape(2048, 256)
        part = jnp.maximum(jnp.dot(rows, weights, preferred_element_type=F32), 0.0)
        hidden[:, cols] = (part * part).astype(BF16)
        return carry

    lax.fori_loop(0, 8, up, 0)

    def down_copy(k, d):
        return to_peer(d, dbuf.at[(x + d) % 4, k], frecv.at[d - 1, k], fs.at[k, d - 1], fr.at[k, d - 1])

    low64 = low

    def collect(k):
        for d in (1, 3, 2):
            down_copy(k, d).wait_recv()
        total = dbuf[x, k].astype(F32)
        for d in range(3):
            total = total + frecv[d, k].astype(F32)
        for b in range(8):
            piece = total[:, (b // 2) * 128 : (b // 2) * 128 + 128]
            if b % 2 == 1:
                piece = pltpu.roll(piece, 64, 1)
            da, db = PLACES[k], PLACES[b % 4]
            stage[slot(da, db) if b < 4 else partner_slot(da, db)] = piece

    needed = {0: rest_down[6:6], 1: rest_down[6:11], 2: rest_down[11:12], 3: rest_down[12:15]}
    for k in range(4):
        for item, da, db in needed[k]:
            take(item, da, db)
        for r in range(4):
            wait_partner(DOWN, k * 4 + r, partner_slot(PLACES[k], PLACES[r]))
        blocks = [wbuf[1, slot(PLACES[k], db)] for db in PLACES]
        blocks += [wbuf[1, partner_slot(PLACES[k], db)] for db in PLACES]
        weights = jnp.concatenate(blocks, axis=0)
        part = nt_dot(hidden[...], weights).astype(BF16)
        for r in range(4):
            dbuf[r, k] = part[r * 64 : (r + 1) * 64, :]
        for d in (2, 1, 3):
            down_copy(k, d).start()
        if k > 0:
            collect(k - 1)
    collect(3)
    for pos in range(16):
        both = jnp.where(low64, stage[2 * pos], pltpu.roll(stage[2 * pos + 1], 64, 1))
        cols = slice(pos * 128, pos * 128 + 128)
        out_ref[:, cols] = (midbuf[:, cols] + both).astype(BF16)

    for item, ev, number, half in sends:
        index = slot(PLACES[ev // 4], PLACES[ev % 4])
        piece = region(item, index, half)
        pltpu.make_async_remote_copy(
            src_ref=piece, dst_ref=piece, send_sem=ssem.at[item, ev, number], recv_sem=rsem.at[item, ev, 0],
            device_id=(partner, x), device_id_type=MESH,
        ).wait_send()
    for item in (KV, UP, DOWN):
        for ev in range(16):
            piece = region(item, slot(PLACES[ev // 4], PLACES[ev % 4]), None)
            pltpu.make_async_remote_copy(
                src_ref=piece, dst_ref=piece, send_sem=psend.at[item, ev], recv_sem=precv.at[item, ev],
                device_id=(partner, x), device_id_type=MESH,
            ).wait_send()
    for d in (1, 2, 3):
        rs_copy(d).wait_send()
        ag_copy(d, False).wait_send()
        for k in range(4):
            down_copy(k, d).wait_send()


def local(
    resid, query_a, key_a, value_a, query_b, key_b, value_b, gain_qa, gain_ka, gain_qb, gain_kb,
    w_out_a, w_out_b, norm_gain, w_up, w_down,
):
    rowtab, coltab = build_tables()
    gains = jnp.stack([jnp.tile(gain_qa, 2), jnp.tile(gain_ka, 2), gain_qb, gain_kb])
    vmem = pl.BlockSpec(memory_space=pltpu.VMEM)
    anywhere = pl.BlockSpec(memory_space=pl.ANY)
    dma = pltpu.SemaphoreType.DMA
    return pl.pallas_call(
        kernel,
        out_shape=jax.ShapeDtypeStruct((64, 2048), BF16),
        in_specs=[vmem] * 10 + [anywhere] * 5,
        out_specs=vmem,
        scratch_shapes=[
            pltpu.VMEM((32, 256, 384), BF16),
            pltpu.VMEM((2, 32, 64, 2048), BF16),
            pltpu.VMEM((2048, 64), BF16),
            pltpu.VMEM((512, 2048), BF16),
            pltpu.VMEM((64, 2048), BF16),
            pltpu.VMEM((1024, 128), BF16),
            pltpu.VMEM((512, 128), BF16),
            pltpu.VMEM((1024, 128), F32),
            pltpu.VMEM((512, 128), F32),
            pltpu.VMEM((1024, 128), F32),
            pltpu.VMEM((512, 256), F32),
            pltpu.VMEM((256, 512), BF16),
            pltpu.VMEM((4, 64, 2048), BF16),
            pltpu.VMEM((3, 64, 2048), BF16),
            pltpu.VMEM((4, 64, 2048), BF16),
            pltpu.VMEM((256, 2048), BF16),
            pltpu.VMEM((4, 4, 64, 512), BF16),
            pltpu.VMEM((3, 4, 64, 512), BF16),
            pltpu.VMEM((32, 64, 128), F32),
            pltpu.VMEM((64, 2048), F32),
            dma((5,)),
            dma((3, 16, 4)),
            dma((3, 16, 2)),
            dma((3, 16)),
            dma((3, 16)),
            dma((2, 3)),
            dma((2, 3)),
            dma((4, 3)),
            dma((4, 3)),
        ],
        compiler_params=pltpu.CompilerParams(
            collective_id=0, has_side_effects=True, vmem_limit_bytes=58 * 1024 * 1024
        ),
    )(
        query_a, key_a, value_a, query_b, key_b, value_b, gains, norm_gain.reshape(1, -1),
        jnp.asarray(rowtab), jnp.asarray(coltab),
        resid, w_out_a, w_out_b, w_up, w_down,
    )


def solution(mesh):
    return jax.shard_map(
        local,
        mesh=mesh,
        in_specs=(
            P(("sp", "tp"), None),
            P("sp", "tp"),
            P("sp", "tp"),
            P("sp", "tp"),
            P("sp", "tp"),
            P("sp", "tp"),
            P("sp", "tp"),
            P(),
            P(),
            P(),
            P(),
            P("tp", None),
            P("tp", None),
            P(),
            P("sp", "tp"),
            P("tp", "sp"),
        ),
        out_specs=P(("sp", "tp"), None),
        check_vma=False,
    )
```

time: 245 us -> 142 us (0.58)
  Pallas kernels: 0 us -> 133 us
  matrix products: 85.7 us -> 0 us
  blocking collectives: 49.9 us -> 0 us
  waiting for transfers between devices: 47.8 us -> 0 us
  other arithmetic: 19.8 us -> 0.59 us
  local copies, waits for them, and re-layouts: 25.1 us -> 7.84 us
  between operations: 13.5 us -> 0.02 us
    pallas_call x0 -> x1, Pallas kernels: none -> 133 us  [local(): pl.pallas_call(kernel, out_shape=jax.ShapeDtypeStruct((64, 2048), BF16),...]
    dot_general x19 -> x0, matrix products: 85.7 us -> none  [the longest x8 37.3 us: fold_block(): jnp.einsum('rkgd,pkd->kgrp', queries, key_block, preferred_element_type=j...]
    all_to_all x3 -> x0, blocking collectives: 49.9 us -> none  [the longest x2 33.6 us: sum_at_owner(): lax.all_to_all(split_up(shard, dim, length), axis, 0, 0, tiled=True)]
    all_gather x3 -> x0, waiting for transfers between devices: 46.6 us -> none  [the longest x1 46.6 us: side_by_side(): result, at, outs = (lax.all_gather(both, axis, axis=dim, tiled=True), 0, [])]
    reduce_sum x15 -> x0, other arithmetic: 10 us -> none  [the longest x8 8.28 us: fold_block(): total = total * factor + jnp.sum(expo, axis=-1)]
    slice x2 -> x0, local copies, waits for them, and re-layouts: 8.29 us -> none  [side_by_side(): outs.append(lax.slice_in_dim(result, at, at + a.shape[along], axis=along))]
    while x41 -> x0, local copies, waits for them, and re-layouts: 7.64 us -> none
    convert_element_type x9 -> x0, other arithmetic: 4.89 us -> none  [the longest x4 2.99 us: norm_rope(): (flat * jnp.cos(angles)[:, None, :] + turned * jnp.sin(angles)[:, None, :...]
  transfers between devices with their start and end apart: 3 -> 0, of which waited for: 1 -> 0; matrix products, arithmetic and copies ran while one was open for 43% -> 0% of each run, Pallas kernels for 0% -> 0%
where the time goes in v1:
time: 142 us; the launch traced here: 141 us
  Pallas kernels  133 us (94%)
  local copies, waits for them, and re-layouts  7.84 us (6%)
    pallas_call x1, Pallas kernels, local(): pl.pallas_call(kernel, out_shape=jax.ShapeDtypeStruct((64, 2048), BF16),...  133 us
    unnamed x14, local copies, waits for them, and re-layouts  7.67 us

profile of v1, /device:TPU:1, one launch (start us, length us, event | category | flops | bytes accessed | tf_op | source)
XLA Modules:
  0.0 141.5 jit_solution(16570623319435568967)
XLA Ops:
  0.0 0.0 copy-start.3
  0.0 0.7 copy-done.3
  0.7 0.0 copy-start.4
  0.7 0.1 stack_tile.6
  0.7 0.6 copy-done.4
  1.3 0.0 copy-start.1
  1.3 0.0 copy-start.2
  1.3 0.1 stack_tile.7
  1.4 0.6 copy-done.1
  2.0 0.0 copy-done.2
  2.0 0.6 pad_maximum_fusion.gains_ref
  2.6 0.0 copy-start
  2.6 1.5 %copy.19.ka_ref = bf16[256,64]{1,0:T(8,128)(2,1)} copy(bf16[256,64]{0,1:T(8,128)(2,1)} %param.20) | data formatting | bytes 65536 | tf_op args[2]
  4.1 0.0 copy-done
  4.1 0.7 copy.20.va_ref
  4.8 2.0 %copy.21.wdown_hbm = bf16[2048,64]{1,0:T(8,128)(2,1)} copy(bf16[2048,64]{0,1:T(8,128)(2,1)} %param.33) | data formatting | bytes 524288 | tf_op args[15]
  6.8 133.0 %shard_map.172 = bf16[64,2048]{1,0:T(8,128)(2,1)} custom-call(bf16[256,256]{1,0:T(8,128)(2,1)} %qa_ref.1, bf16[256,64]{1,0:T(8,128)(2,1)} %copy.19.ka_ref, bf16[256,64]{1,0:T(8,128)(2,1)} %copy.20.va_ref, bf16[256,256]{1,0:T(8,128)(2,1)} %qb_ref.1, bf16[256,128]{1,0:T(8,128)(2,1)} %kb_ref.1, bf16[256,128]{1,0:T(8,128)(2,1)} %vb_ref.1, ...), custom_call_target="tpu_custom_call" | custom-call | tf_op jit(solution)/shard_map/pallas_call | solution.py:452
  139.8 1.7 %copy.23 = bf16[64,2048]{1,0:T(8,128)(2,1)} copy(bf16[64,2048]{1,0:T(8,128)(2,1)} %shard_map.172) | data formatting | bytes 524288
  (2 shorter events, 0.0 us)
Async XLA Ops:
  0.0 0.7 copy-start.3
  0.7 0.7 copy-start.4
  1.3 0.7 copy-start.1
  1.3 0.7 copy-start.2
  2.6 1.5 %copy-start = (bf16[256,64]{0,1:T(8,128)(2,1)S(1)}, bf16[256,64]{0,1:T(8,128)(2,1)}, u32[]{:S(2)}) copy-start(bf16[256,64]{0,1:T(8,128)(2,1)} %param.21) | copy-start | bytes 98308

commit v2 on v1

v2 whole, which is shorter than its diff:
```python
import functools
import math

import jax
import jax.numpy as jnp
import numpy as np
from jax import lax
from jax.experimental import pallas as pl
from jax.experimental.pallas import tpu as pltpu
from jax.sharding import PartitionSpec as P

MESH = pl.DeviceIdType.MESH
EPS = 1e-06
F32 = jnp.float32
BF16 = jnp.bfloat16
LOG2E = 1.4426950408889634
KV, UP, DOWN = 0, 1, 2
ORDER = (
    (0, 0), (3, 0), (1, 0), (0, 3), (0, 1), (2, 0), (3, 3), (3, 1),
    (1, 3), (1, 1), (0, 2), (2, 3), (2, 1), (3, 2), (1, 2), (2, 2),
)


def build_tables():
    rows, cols = [], []
    for width in (64, 128):
        quarter = width // 4
        freqs = (10000.0 ** (-(2.0 * np.arange(quarter)) / (width // 2))).astype(np.float32)
        freqs = np.concatenate([freqs, freqs])
        entry = np.arange(width)
        sign = np.where((entry // quarter) % 2 == 0, -1.0, 1.0)

        def pair(count, low):
            ang = (np.arange(count, dtype=np.float32)[:, None] * freqs).astype(np.float64)
            full = np.zeros((2, count, width))
            half = slice(0, width // 2) if low else slice(width // 2, width)
            full[0][:, half] = np.cos(ang)
            full[1][:, half] = np.sin(ang)
            full[1] *= sign
            return np.tile(full, (1, 1, 128 // width)).astype(np.float32)

        rows.append(pair(128, True))
        cols.append(pair(64, False))
    row = np.concatenate(rows, axis=0)
    row = row.reshape(4, 32, 4, 128).transpose(1, 0, 2, 3).reshape(32, 16, 128)
    col = np.concatenate(cols, axis=0)
    return row, col


def nt_dot(a, b):
    return lax.dot_general(a, b, (((1,), (1,)), ((), ())), preferred_element_type=F32)


def nn_dot(a, b):
    return jnp.dot(a, b, preferred_element_type=F32)


def pick(i, values):
    result = jnp.int32(values[0])
    for number, value in enumerate(values[1:]):
        result = jnp.where(i == number + 1, jnp.int32(value), result)
    return result


PLAN = {
    1: [(0, 1), (0, 2)],
    2: [(0, 3)],
    3: [(0, 4)],
    4: [(0, 5)],
    5: [(0, 6)],
    6: [(0, 7)],
    7: [(0, 8)],
    8: [(0, 9), (1, "b")],
    9: [(0, 10)],
    10: [(0, 11)],
    11: [(0, 12), (1, 1), (1, 2)],
    12: [(0, 13)],
    13: [(0, 14)],
    14: [(1, 5), (1, 3), (1, 4), (0, 15)],
    15: [],
    16: [],
}
AFTER_PROJECT = [(1, 6), (2, "b"), (1, 7), (2, "a"), "combine", (1, 8), (1, 9), (1, 11), (1, 12), (2, 1), (2, 2), (1, 10)]
AFTER_SUM = [(2, 5), (2, 4), (1, 13), "relay", (2, 3), (1, 14), (1, 15), (2, 6), (2, 7)]
AMID_UP = [(2, 8), (2, 9)]
BEFORE_DOWN = {0: [], 1: [(2, 11), (2, 12)], 2: [(2, 10)], 3: [(2, 13), (2, 14), (2, 15)]}


def kernel(
    qa_ref, ka_ref, va_ref, qb_ref, kb_ref, vb_ref, gqa_ref, gka_ref, gqb_ref, gkb_ref,
    ngain_ref, rowtab_ref, coltab_ref,
    resid_hbm, woa_hbm, wob_hbm, wup_hbm, wdown_hbm,
    out_ref,
    kvbuf, wbuf, wo, resid, qa, qb, s_even, s_odd, tops, acc_a, acc_b, attn,
    pout, phalf, rsbuf, nbuf, hidden, dbuf, dhalf, frecv, stage, midbuf,
    lsem, ssem, rsem, psend, precv, xs, xr, gs, gr,
):
    sp = lax.axis_index("sp")
    x = lax.axis_index("tp")
    z, y, c = sp // 8, (sp // 2) % 4, sp % 2
    n = 1 - c
    partner = z * 8 + y * 2 + n

    def slot(da, db):
        return ((z + n * db + c * da) % 4) * 8 + ((y + n * da + c * db) % 4) * 2 + c

    def partner_slot(da, db):
        return ((z + c * db + n * da) % 4) * 8 + ((y + c * da + n * db) % 4) * 2 + n

    def event(da, db):
        return ORDER.index((da, db))

    barrier = pltpu.get_barrier_semaphore()
    others = [(slot(1, 0), x), (slot(3, 0), x), (slot(0, 1), x), (slot(0, 3), x), (partner, x)]
    others += [(sp, (x + d) % 4) for d in (1, 3)]
    for dev in others:
        pl.semaphore_signal(barrier, inc=1, device_id=dev, device_id_type=MESH)

    loads = [
        pltpu.make_async_copy(wup_hbm, wbuf.at[0, sp], lsem.at[0]),
        pltpu.make_async_copy(wdown_hbm, wbuf.at[1, sp], lsem.at[1]),
        pltpu.make_async_copy(woa_hbm, wo.at[pl.ds(0, 256)], lsem.at[2]),
        pltpu.make_async_copy(wob_hbm, wo.at[pl.ds(256, 256)], lsem.at[3]),
        pltpu.make_async_copy(resid_hbm, resid, lsem.at[4]),
    ]
    for load in loads:
        load.start()

    def region(item, index, half):
        if item == KV:
            ref, size = kvbuf.at[index], 384
        else:
            ref, size = wbuf.at[item - 1, index], 32
        if half is None:
            return ref
        return ref.at[pl.ds(half * size, size)]

    sends = []

    def send(item, ev, number, index, half, to, there):
        piece = region(item, index, half)
        copy = pltpu.make_async_remote_copy(
            src_ref=piece,
            dst_ref=piece,
            send_sem=ssem.at[item, ev, number],
            recv_sem=rsem.at[item, event(*there), 0 if half is None else half],
            device_id=(slot(*to), x),
            device_id_type=MESH,
        )
        copy.start()
        sends.append((item, ev, number, half))

    def hand_over(item, ev, index):
        piece = region(item, index, None)
        pltpu.make_async_remote_copy(
            src_ref=piece,
            dst_ref=piece,
            send_sem=psend.at[item, ev],
            recv_sem=precv.at[item, ev],
            device_id=(partner, x),
            device_id_type=MESH,
        ).start()

    def wait_in(item, ev, index, half):
        piece = region(item, index, half)
        pltpu.make_async_remote_copy(
            src_ref=piece,
            dst_ref=piece,
            send_sem=ssem.at[item, ev, 0],
            recv_sem=rsem.at[item, ev, 0 if half is None else half],
            device_id=(partner, x),
            device_id_type=MESH,
        ).wait_recv()

    def wait_partner(item, ev, index):
        piece = region(item, index, None)
        pltpu.make_async_remote_copy(
            src_ref=piece,
            dst_ref=piece,
            send_sem=psend.at[item, ev],
            recv_sem=precv.at[item, ev],
            device_id=(partner, x),
            device_id_type=MESH,
        ).wait_recv()

    def take(item, number):
        with jax.named_scope(f"take{item}_{number}"):
            if number in ("a", "b"):
                start_own(item, number)
            else:
                take_in(item, *ORDER[number])

    def start_own(item, ring):
        index = slot(0, 0)
        if ring == "a":
            send(item, 0, 0, index, None, (1, 0), (3, 0))
            send(item, 0, 1, index, None, (3, 0), (1, 0))
        else:
            send(item, 0, 2, index, None, (0, 1), (0, 3))
            send(item, 0, 3, index, None, (0, 3), (0, 1))
            hand_over(item, 0, index)

    def take_in(item, da, db):
        ev, index = event(da, db), slot(da, db)
        if da == 0 and db == 0:
            raise ValueError(item)
        elif db == 0:
            if da == 2:
                wait_in(item, ev, index, 0)
                wait_in(item, ev, index, 1)
            else:
                wait_in(item, ev, index, None)
                if da == 3:
                    send(item, ev, 0, index, 0, (1, 0), (2, 0))
                else:
                    send(item, ev, 0, index, 1, (3, 0), (2, 0))
            send(item, ev, 2, index, None, (0, 1), (da, 3))
            send(item, ev, 3, index, None, (0, 3), (da, 1))
        elif db == 2:
            wait_in(item, ev, index, 0)
            wait_in(item, ev, index, 1)
        else:
            wait_in(item, ev, index, None)
            if db == 3:
                send(item, ev, 0, index, 0, (0, 1), (da, 2))
            else:
                send(item, ev, 0, index, 1, (0, 3), (da, 2))
        hand_over(item, ev, index)

    lane = lax.broadcasted_iota(jnp.int32, (64, 128), 1)
    low = lane < 64
    rowtab = rowtab_ref[sp]

    def both_heads(ref):
        return jnp.concatenate([ref[...], ref[...]], axis=1)

    def rotate(v, gain, width, r, s):
        quarter = width // 4
        kind = 0 if width == 64 else 2

        def angles(which):
            across = rowtab[which * 4 + r : which * 4 + r + 1]
            if s != r:
                across = jnp.where(low[0:1], across, rowtab[which * 4 + s : which * 4 + s + 1])
            return across + coltab_ref[which]

        sq = v * v
        if width == 64:
            left = jnp.sum(jnp.where(low, sq, 0.0), axis=-1, keepdims=True)
            right = jnp.sum(jnp.where(low, 0.0, sq), axis=-1, keepdims=True)
            mean = jnp.where(low, left, right) * (1.0 / 64)
        else:
            mean = jnp.sum(sq, axis=-1, keepdims=True) * (1.0 / 128)
        u = v * lax.rsqrt(mean + EPS) * gain
        even = (lane // quarter) % 2 == 0
        turned = jnp.where(even, pltpu.roll(u, 128 - quarter, 1), pltpu.roll(u, quarter, 1))
        return u * angles(kind) + turned * angles(kind + 1)

    own = slot(0, 0)
    turned = ka_ref[...].astype(F32)
    turned = jnp.concatenate([turned[:, 0:128], turned[:, 128:256]], axis=0).T
    gain = both_heads(gka_ref)
    for r in range(2):
        block = rotate(turned[r * 64 : (r + 1) * 64], gain, 64, r, r + 2)
        kvbuf[own, r * 64 : (r + 1) * 64, :] = block.astype(BF16)
    for r in range(4):
        block = rotate(kb_ref[r * 64 : (r + 1) * 64, :].astype(F32), gkb_ref[...], 128, r, r)
        kvbuf[own, 128 + r * 64 : 192 + r * 64, :] = block.astype(BF16)
    for half in range(2):
        tokens = slice(half * 128, half * 128 + 128)
        kvbuf[own, 384 + half * 64 : 448 + half * 64, :] = va_ref[:, tokens]
        kvbuf[own, 512 + half * 128 : 640 + half * 128, :] = vb_ref[tokens, :].astype(F32).T.astype(BF16)

    with jax.named_scope("barrier"):
        pl.semaphore_wait(barrier, len(others))
    take(KV, "a")
    take(KV, "b")
    loads[0].wait()
    take(UP, "a")

    with jax.named_scope("queries"):
        gain_a = both_heads(gqa_ref)
        for g in range(2):
            lanes = slice(g * 128, g * 128 + 128)
            rows = [slice(r * 64, r * 64 + 64) for r in range(4)]
            heads = [rotate(qa_ref[rows[r], lanes].astype(F32), gain_a, 64, r, r) for r in range(4)]
            heads = jnp.concatenate(heads, axis=0).T.astype(BF16)
            for h in range(2):
                head = heads[h * 64 : h * 64 + 64]
                qa[2 * g + h, 0:64, 0:256] = head
                qa[2 * g + h, 0:64, 256:512] = jnp.zeros_like(head)
                qa[2 * g + h, 64:128, 0:256] = jnp.zeros_like(head)
                qa[2 * g + h, 64:128, 256:512] = head
            heads = [rotate(qb_ref[rows[r], lanes].astype(F32), gqb_ref[...], 128, r, r) for r in range(4)]
            qb[g] = jnp.concatenate(heads, axis=0).T.astype(BF16)
        tops[...] = jnp.full_like(tops, -1e30)
        acc_a[...] = jnp.zeros_like(acc_a)
        acc_b[...] = jnp.zeros_like(acc_b)

    scale_a = 64 ** (-0.5) * LOG2E
    scale_b = 128 ** (-0.5) * LOG2E

    def turned_values(pieces):
        values = jnp.concatenate(pieces, axis=1)
        return jnp.concatenate([values, jnp.ones((16, 512), BF16)], axis=0)

    def score(pair, target):
        keys_a = jnp.concatenate([kvbuf[s, 0:128, :] for s in pair], axis=0)
        keys_b = jnp.concatenate([kvbuf[s, 128:384, :] for s in pair], axis=0)

        def one(h):
            if h < 4:
                scores = nn_dot(keys_a, qa[h]) * scale_a
                scores = jnp.concatenate([scores[:, 0:256], scores[:, 256:512]], axis=0)
            else:
                scores = nn_dot(keys_b, qb[h - 4]) * scale_b
            target[h] = scores
            before = tops[h, 0:1, :]
            top = jnp.maximum(before, jnp.max(scores, axis=0, keepdims=True))
            tops[h, 0:1, :] = top
            tops[h, 1:2, :] = jnp.exp2(before - top)

        return one

    def gather_values(pair):
        def one(h):
            if h < 4:
                return turned_values([kvbuf[s, 384 + 64 * half : 448 + 64 * half, :] for half in range(2) for s in pair])
            return turned_values([kvbuf[s, 512 + 128 * half : 640 + 128 * half, :] for s in pair for half in range(2)])

        return one(0), one(4)

    def use(source, h, values, top, factor):
        expo = jnp.exp2(source[h] - top).astype(BF16)
        got = nn_dot(values[0] if h < 4 else values[1], expo)
        acc, index = (acc_a, h) if h < 4 else (acc_b, h - 4)
        acc[index] = acc[index] * factor + got

    def both(now, after, source, target):
        values = gather_values(now)
        scorer = None if after is None else score(after, target)
        for h in range(6):
            top, factor = tops[h, 0:1, :], tops[h, 1:2, :]
            if scorer is not None:
                scorer(h)
            use(source, h, values, top, factor)

    def my_block(t, shift):
        places = ORDER[shift::2]
        return slot(pick(t, [p[0] for p in places]), pick(t, [p[1] for p in places]))

    def partner_block(t, shift):
        places = ORDER[shift::2]
        return partner_slot(pick(t, [p[0] for p in places]), pick(t, [p[1] for p in places]))

    def ready(t, shift):
        for number in range(6):
            if PLAN.get(2 * number + shift):

                @pl.when(t == number)
                def _(number=number):
                    for what in PLAN[2 * number + shift]:
                        take(*what)

    def fetch(number, t, shift):
        theirs = partner_block(t, shift - 1)
        with jax.named_scope("pwait"):
            wait_partner(KV, number - 1, theirs)
        return my_block(t, shift + 1), theirs

    def attend(t, pair):
        with jax.named_scope("step"):
            ready(t, 2)
            middle = fetch(2 * t + 2, t, 2)
            both(pair, middle, s_odd, s_even)
            ready(t, 3)
            after = fetch(2 * t + 3, t, 3)
            both(middle, after, s_even, s_odd)
        return after

    loads[1].wait()
    with jax.named_scope("first"):
        wait_partner(KV, 0, partner)
        pair = (own, partner)
        first = score(pair, s_even)
        for h in range(6):
            first(h)
        for what in PLAN[1]:
            take(*what)
        after = (slot(*ORDER[1]), slot(*ORDER[2]))
        both(pair, after, s_even, s_odd)
    pair = lax.fori_loop(0, 6, attend, after)
    with jax.named_scope("laststep"):
        for what in PLAN[14]:
            take(*what)
        theirs = partner_slot(*ORDER[13])
        wait_partner(KV, 13, theirs)
        middle = (slot(*ORDER[15]), theirs)
        both(pair, middle, s_odd, s_even)
        for what in PLAN[15]:
            take(*what)
        after = (partner_slot(*ORDER[14]), partner_slot(*ORDER[15]))
        wait_partner(KV, 14, after[0])
        wait_partner(KV, 15, after[1])
        both(middle, after, s_even, s_odd)
        both(after, None, s_odd, None)
        for what in PLAN[16]:
            take(*what)

    for h in range(4):
        acc = acc_a[h]
        acc_a[h, 0:64, :] = acc[0:64] / acc[64:65]
    for g in range(2):
        both_rows = jnp.concatenate([acc_a[2 * g, 0:64, :], acc_a[2 * g + 1, 0:64, :]], axis=0)
        attn[:, g * 128 : (g + 1) * 128] = both_rows.T.astype(BF16)
        acc = acc_b[g]
        attn[:, 256 + g * 128 : 256 + (g + 1) * 128] = (acc[0:128] / acc[128:129]).T.astype(BF16)
    loads[2].wait()
    loads[3].wait()

    def project(j, carry):
        cols = pl.ds(pl.multiple_of(j * 512, 512), 512)
        part = jnp.dot(attn[...], wo[:, cols], preferred_element_type=F32).astype(BF16)
        for r in range(4):
            pout[r, :, cols] = part[r * 64 : (r + 1) * 64, :]
        return carry

    with jax.named_scope("project"):
        lax.fori_loop(0, 4, project, 0)

    def to_peer(forward, src, dst, send_sem, recv_sem):
        return pltpu.make_async_remote_copy(
            src_ref=src,
            dst_ref=dst,
            send_sem=send_sem,
            recv_sem=recv_sem,
            device_id=(sp, (x + (1 if forward else 3)) % 4),
            device_id_type=MESH,
        )

    class TpSum:
        def __init__(self, number, blocks, halves, received):
            self.number, self.blocks, self.halves, self.received = number, blocks, halves, received
            width = received(0).shape[1] // 2
            self.parts = (pl.ds(0, width), pl.ds(width, width))

        def copy(self, kind, way):
            near = self.blocks((x + (1, 3)[way]) % 4)
            if kind == 0:
                src, dst = self.blocks((x + 2) % 4).at[:, self.parts[way]], self.halves(way)
            else:
                part = self.parts[1 - way] if kind == 1 else self.parts[way]
                src, dst = near.at[:, part], self.received(way).at[:, part]
            return to_peer(way == 0, src, dst, xs.at[self.number, kind, way], xr.at[self.number, kind, way])

        def start(self):
            for kind in (0, 1):
                for way in (0, 1):
                    self.copy(kind, way).start()

        def combine(self):
            for way in (0, 1):
                self.copy(0, way).wait_recv()
                near, part = self.blocks((x + (1, 3)[way]) % 4), self.parts[way]
                near[:, part] = (near[:, part].astype(F32) + self.halves(way)[...].astype(F32)).astype(BF16)
                self.copy(2, way).start()

        def total(self):
            for kind in (1, 2):
                for way in (0, 1):
                    self.copy(kind, way).wait_recv()
            return self.blocks(x)[...].astype(F32) + self.received(0)[...].astype(F32) + self.received(1)[...].astype(F32)

        def drain(self):
            for kind in (0, 1, 2):
                for way in (0, 1):
                    self.copy(kind, way).wait_send()

    proj = TpSum(0, lambda r: pout.at[r], lambda w: phalf.at[w], lambda w: rsbuf.at[w])
    proj.start()
    for what in AFTER_PROJECT:
        if what == "combine":
            with jax.named_scope("combine"):
                proj.combine()
        else:
            take(*what)
    loads[4].wait()
    with jax.named_scope("rswait"):
        total = proj.total()
    mid = (resid[...].astype(F32) + total).astype(BF16).astype(F32)
    midbuf[...] = mid
    norm = mid * lax.rsqrt(jnp.mean(mid * mid, axis=-1, keepdims=True) + EPS) * ngain_ref[...]
    nbuf[x] = norm.astype(BF16)

    halves = (pl.ds(0, 1024), pl.ds(1024, 1024))

    def rows_copy(kind, way, arriving):
        hops = (1 if kind < 2 else 2) if arriving else (0 if kind < 2 else 1)
        block = (x + 4 - hops) % 4 if way == 0 else (x + hops) % 4
        part = halves[1 - way] if kind == 1 else halves[way]
        piece = nbuf.at[block, :, part]
        return to_peer(way == 0, piece, piece, gs.at[kind, way], gr.at[kind, way])

    for kind in (0, 1):
        for way in (0, 1):
            rows_copy(kind, way, False).start()
    for what in AFTER_SUM:
        if what == "relay":
            with jax.named_scope("relay"):
                for way in (0, 1):
                    rows_copy(0, way, True).wait_recv()
                    rows_copy(2, way, False).start()
        else:
            take(*what)
    with jax.named_scope("upwait"):
        for ev in range(16):
            wait_partner(UP, ev, partner_slot(*ORDER[ev]))
    with jax.named_scope("rowswait"):
        for kind in (1, 2):
            for way in (0, 1):
                rows_copy(kind, way, True).wait_recv()

    def up(j, carry):
        cols = pl.ds(pl.multiple_of(j * 256, 256), 256)
        rows = nbuf[...].reshape(256, 2048)
        weights = wbuf[0, :, :, cols].reshape(2048, 256)
        part = jnp.maximum(jnp.dot(rows, weights, preferred_element_type=F32), 0.0)
        hidden[:, cols] = (part * part).astype(BF16)
        return carry

    with jax.named_scope("up"):
        lax.fori_loop(0, 4, up, 0)
    for what in AMID_UP:
        take(*what)
    with jax.named_scope("up"):
        lax.fori_loop(4, 8, up, 0)

    sums = [
        TpSum(k + 1, lambda r, k=k: dbuf.at[r, k], lambda w, k=k: dhalf.at[k, w], lambda w, k=k: frecv.at[k, w])
        for k in range(4)
    ]

    low64 = low

    def collect(k):
        total = sums[k].total()
        for b in range(8):
            piece = total[:, (b // 2) * 128 : (b // 2) * 128 + 128]
            if b % 2 == 1:
                piece = pltpu.roll(piece, 64, 1)
            place = ORDER[4 * k + b % 4]
            stage[slot(*place) if b < 4 else partner_slot(*place)] = piece

    for k in range(4):
        for what in BEFORE_DOWN[k]:
            take(*what)
        places = ORDER[4 * k : 4 * k + 4]
        for r in range(4):
            wait_partner(DOWN, k * 4 + r, partner_slot(*places[r]))
        blocks = [wbuf[1, slot(*place)] for place in places]
        blocks += [wbuf[1, partner_slot(*place)] for place in places]
        weights = jnp.concatenate(blocks, axis=0)
        with jax.named_scope(f"down{k}"):
            part = nt_dot(hidden[...], weights).astype(BF16)
            for r in range(4):
                dbuf[r, k] = part[r * 64 : (r + 1) * 64, :]
        sums[k].start()
        if k > 0:
            with jax.named_scope(f"combine{k - 1}"):
                sums[k - 1].combine()
        if k > 1:
            with jax.named_scope(f"collect{k - 2}"):
                collect(k - 2)
    with jax.named_scope("combine3"):
        sums[3].combine()
    with jax.named_scope("collect23"):
        collect(2)
        collect(3)
    for pos in range(16):
        both = jnp.where(low64, stage[2 * pos], pltpu.roll(stage[2 * pos + 1], 64, 1))
        cols = slice(pos * 128, pos * 128 + 128)
        out_ref[:, cols] = (midbuf[:, cols] + both).astype(BF16)

    for item, ev, number, half in sends:
        index = slot(*ORDER[ev])
        piece = region(item, index, half)
        pltpu.make_async_remote_copy(
            src_ref=piece, dst_ref=piece, send_sem=ssem.at[item, ev, number], recv_sem=rsem.at[item, ev, 0],
            device_id=(partner, x), device_id_type=MESH,
        ).wait_send()
    for item in (KV, UP, DOWN):
        for ev in range(16):
            piece = region(item, slot(*ORDER[ev]), None)
            pltpu.make_async_remote_copy(
                src_ref=piece, dst_ref=piece, send_sem=psend.at[item, ev], recv_sem=precv.at[item, ev],
                device_id=(partner, x), device_id_type=MESH,
            ).wait_send()
    for sum_over in [proj] + sums:
        sum_over.drain()
    for kind in (0, 1, 2):
        for way in (0, 1):
            rows_copy(kind, way, False).wait_send()


def local(
    resid, query_a, key_a, value_a, query_b, key_b, value_b, gain_qa, gain_ka, gain_qb, gain_kb,
    w_out_a, w_out_b, norm_gain, w_up, w_down,
):
    rowtab, coltab = build_tables()
    vmem = pl.BlockSpec(memory_space=pltpu.VMEM)
    anywhere = pl.BlockSpec(memory_space=pl.ANY)
    dma = pltpu.SemaphoreType.DMA
    return pl.pallas_call(
        kernel,
        out_shape=jax.ShapeDtypeStruct((64, 2048), BF16),
        in_specs=[vmem] * 13 + [anywhere] * 5,
        out_specs=vmem,
        scratch_shapes=[
            pltpu.VMEM((32, 768, 128), BF16),
            pltpu.VMEM((2, 32, 64, 2048), BF16),
            pltpu.VMEM((512, 2048), BF16),
            pltpu.VMEM((64, 2048), BF16),
            pltpu.VMEM((4, 128, 512), BF16),
            pltpu.VMEM((2, 128, 256), BF16),
            pltpu.VMEM((6, 512, 256), F32),
            pltpu.VMEM((6, 512, 256), F32),
            pltpu.VMEM((6, 8, 256), F32),
            pltpu.VMEM((4, 80, 256), F32),
            pltpu.VMEM((2, 144, 256), F32),
            pltpu.VMEM((256, 512), BF16),
            pltpu.VMEM((4, 64, 2048), BF16),
            pltpu.VMEM((2, 64, 1024), BF16),
            pltpu.VMEM((2, 64, 2048), BF16),
            pltpu.VMEM((4, 64, 2048), BF16),
            pltpu.VMEM((256, 2048), BF16),
            pltpu.VMEM((4, 4, 64, 512), BF16),
            pltpu.VMEM((4, 2, 64, 256), BF16),
            pltpu.VMEM((4, 2, 64, 512), BF16),
            pltpu.VMEM((32, 64, 128), F32),
            pltpu.VMEM((64, 2048), F32),
            dma((5,)),
            dma((3, 16, 4)),
            dma((3, 16, 2)),
            dma((3, 16)),
            dma((3, 16)),
            dma((5, 3, 2)),
            dma((5, 3, 2)),
            dma((3, 2)),
            dma((3, 2)),
        ],
        compiler_params=pltpu.CompilerParams(
            collective_id=0, has_side_effects=True, vmem_limit_bytes=58 * 1024 * 1024
        ),
    )(
        query_a, key_a.T, value_a.T, query_b, key_b, value_b,
        gain_qa.reshape(1, -1), gain_ka.reshape(1, -1), gain_qb.reshape(1, -1), gain_kb.reshape(1, -1),
        norm_gain.reshape(1, -1), jnp.asarray(rowtab), jnp.asarray(coltab),
        resid, w_out_a, w_out_b, w_up, w_down.T,
    )


def solution(mesh):
    return jax.shard_map(
        local,
        mesh=mesh,
        in_specs=(
            P(("sp", "tp"), None),
            P("sp", "tp"),
            P("sp", "tp"),
            P("sp", "tp"),
            P("sp", "tp"),
            P("sp", "tp"),
            P("sp", "tp"),
            P(),
            P(),
            P(),
            P(),
            P("tp", None),
            P("tp", None),
            P(),
            P("sp", "tp"),
            P("tp", "sp"),
        ),
        out_specs=P(("sp", "tp"), None),
        check_vma=False,
    )
```

time: 142 us -> 87.9 us (0.62)
  Pallas kernels: 133 us -> 86.1 us
  local copies, waits for them, and re-layouts: 7.84 us -> 1.67 us
    pallas_call x1, Pallas kernels: 133 us -> 86.1 us  [local(): pl.pallas_call(kernel, out_shape=jax.ShapeDtypeStruct((64, 2048), BF16),...]
    unnamed x14 -> x1, local copies, waits for them, and re-layouts: 7.67 us -> 1.67 us
where the time goes in v2:
time: 87.9 us; the launch traced here: 87.8 us
  Pallas kernels  86.1 us (98%)
  local copies, waits for them, and re-layouts  1.67 us (2%)
    pallas_call x1, Pallas kernels, local(): pl.pallas_call(kernel, out_shape=jax.ShapeDtypeStruct((64, 2048), BF16),...  86.1 us

profile of v2, /device:TPU:1, one launch (start us, length us, event | category | flops | bytes accessed | tf_op | source)
XLA Modules:
  0.0 87.8 jit_solution(4239523087855338275)
XLA Ops:
  0.0 86.1 %shard_map.172 = bf16[64,2048]{1,0:T(8,128)(2,1)} custom-call(bf16[256,256]{1,0:T(8,128)(2,1)} %qa_ref.1, bf16[64,256]{1,0:T(8,128)(2,1)} %bitcast.9, bf16[64,256]{1,0:T(8,128)(2,1)} %bitcast.10, bf16[256,256]{1,0:T(8,128)(2,1)} %qb_ref.1, bf16[256,128]{1,0:T(8,128)(2,1)} %kb_ref.1, bf16[256,128]{1,0:T(8,128)(2,1)} %vb_ref.1, f32[1,64]{1,0:T(1,128)} %bitcast.12, ...), custom_call_target="tpu_custom_call" | custom-call | tf_op jit(solution)/shard_map/pallas_call | solution.py:613
  86.1 1.7 %copy.20 = bf16[64,2048]{1,0:T(8,128)(2,1)} copy(bf16[64,2048]{1,0:T(8,128)(2,1)} %shard_map.172) | data formatting | bytes 524288

commit v3 on v2

--- a/solution.py
+++ b/solution.py
@@ -63,27 +63,26 @@
 
 
 PLAN = {
-    1: [(0, 1), (0, 2)],
-    2: [(0, 3)],
-    3: [(0, 4)],
+    1: [(0, 1), (0, 2), (0, 3), (0, 4)],
     4: [(0, 5)],
-    5: [(0, 6)],
-    6: [(0, 7)],
-    7: [(0, 8)],
-    8: [(0, 9), (1, "b")],
-    9: [(0, 10)],
-    10: [(0, 11)],
-    11: [(0, 12), (1, 1), (1, 2)],
-    12: [(0, 13)],
-    13: [(0, 14)],
-    14: [(1, 5), (1, 3), (1, 4), (0, 15)],
+    5: [(0, 6), (0, 7)],
+    7: [(0, 8), (0, 9)],
+    8: [(0, 10)],
+    10: [(0, 11), (0, 12)],
+    11: [(0, 13), (1, "b")],
+    12: [(0, 14)],
+    14: [(0, 15), (1, 1), (1, 2)],
     15: [],
-    16: [],
+    16: [(1, 3), (1, 4)],
 }
-AFTER_PROJECT = [(1, 6), (2, "b"), (1, 7), (2, "a"), "combine", (1, 8), (1, 9), (1, 11), (1, 12), (2, 1), (2, 2), (1, 10)]
-AFTER_SUM = [(2, 5), (2, 4), (1, 13), "relay", (2, 3), (1, 14), (1, 15), (2, 6), (2, 7)]
-AMID_UP = [(2, 8), (2, 9)]
-BEFORE_DOWN = {0: [], 1: [(2, 11), (2, 12)], 2: [(2, 10)], 3: [(2, 13), (2, 14), (2, 15)]}
+AFTER_PROJECT = [(1, 5), (1, 6), (1, 7), "combine", (1, 8), (1, 9), (2, "a"), (2, "b"), (1, 10)]
+AFTER_SUM = [(1, 11), (1, 12), (2, 1), (2, 2), (1, 13), (1, 14), "relay", (2, 5), (2, 3), (2, 4), (1, 15)]
+AMID_UP = [(2, 6), (2, 7)]
+CHUNKS = ((0, 4), (4, 8), (8, 12), (12, 16))
+TAIL = [
+    "down0", (2, 8), (2, 9), "down1", (2, 11), (2, 12), "combine0", (2, 10), "down2", (2, 13), (2, 14), (2, 15), "combine1", "collect0",
+    "down3", "combine2", "collect1", "combine3", "collect2", "collect3",
+]
 
 
 def kernel(
@@ -93,7 +92,7 @@
     out_ref,
     kvbuf, wbuf, wo, resid, qa, qb, s_even, s_odd, tops, acc_a, acc_b, attn,
     pout, phalf, rsbuf, nbuf, hidden, dbuf, dhalf, frecv, stage, midbuf,
-    lsem, ssem, rsem, psend, precv, xs, xr, gs, gr,
+    lsem, ssem, rsem, precv, xs, xr, gs, gr,
 ):
     sp = lax.axis_index("sp")
     x = lax.axis_index("tp")
@@ -135,53 +134,26 @@
             return ref
         return ref.at[pl.ds(half * size, size)]
 
-    sends = []
-
-    def send(item, ev, number, index, half, to, there):
-        piece = region(item, index, half)
-        copy = pltpu.make_async_remote_copy(
-            src_ref=piece,
-            dst_ref=piece,
-            send_sem=ssem.at[item, ev, number],
-            recv_sem=rsem.at[item, event(*there), 0 if half is None else half],
-            device_id=(slot(*to), x),
-            device_id_type=MESH,
+    def block_copy(item, piece, recv_sem, to):
+        return pltpu.make_async_remote_copy(
+            src_ref=piece, dst_ref=piece, send_sem=ssem.at[item], recv_sem=recv_sem, device_id=(to, x), device_id_type=MESH,
         )
-        copy.start()
-        sends.append((item, ev, number, half))
+
+    def send(item, index, half, to, there):
+        block_copy(item, region(item, index, half), rsem.at[item, event(*there)], slot(*to)).start()
 
     def hand_over(item, ev, index):
-        piece = region(item, index, None)
-        pltpu.make_async_remote_copy(
-            src_ref=piece,
-            dst_ref=piece,
-            send_sem=psend.at[item, ev],
-            recv_sem=precv.at[item, ev],
-            device_id=(partner, x),
-            device_id_type=MESH,
-        ).start()
-
-    def wait_in(item, ev, index, half):
-        piece = region(item, index, half)
-        pltpu.make_async_remote_copy(
-            src_ref=piece,
-            dst_ref=piece,
-            send_sem=ssem.at[item, ev, 0],
-            recv_sem=rsem.at[item, ev, 0 if half is None else half],
-            device_id=(partner, x),
-            device_id_type=MESH,
-        ).wait_recv()
+        block_copy(item, region(item, index, None), precv.at[item, ev], partner).start()
+
+    def wait_in(item, ev, index):
+        block_copy(item, region(item, index, None), rsem.at[item, ev], partner).wait_recv()
 
     def wait_partner(item, ev, index):
-        piece = region(item, index, None)
-        pltpu.make_async_remote_copy(
-            src_ref=piece,
-            dst_ref=piece,
-            send_sem=psend.at[item, ev],
-            recv_sem=precv.at[item, ev],
-            device_id=(partner, x),
-            device_id_type=MESH,
-        ).wait_recv()
+        block_copy(item, region(item, index, None), precv.at[item, ev], partner).wait_recv()
+
+    def drain(item):
+        ref = kvbuf.at[pl.ds(0, 31)] if item == KV else wbuf.at[item - 1, pl.ds(0, 31)]
+        block_copy(item, ref, rsem.at[item, 0], partner).wait_send()
 
     def take(item, number):
         with jax.named_scope(f"take{item}_{number}"):
@@ -193,39 +165,36 @@
     def start_own(item, ring):
         index = slot(0, 0)
         if ring == "a":
-            send(item, 0, 0, index, None, (1, 0), (3, 0))
-            send(item, 0, 1, index, None, (3, 0), (1, 0))
+            send(item, index, None, (1, 0), (3, 0))
+            send(item, index, None, (3, 0), (1, 0))
         else:
-            send(item, 0, 2, index, None, (0, 1), (0, 3))
-            send(item, 0, 3, index, None, (0, 3), (0, 1))
+            send(item, index, None, (0, 1), (0, 3))
+            send(item, index, None, (0, 3), (0, 1))
             hand_over(item, 0, index)
 
     def take_in(item, da, db):
         ev, index = event(da, db), slot(da, db)
-        if da == 0 and db == 0:
-            raise ValueError(item)
-        elif db == 0:
-            if da == 2:
-                wait_in(item, ev, index, 0)
-                wait_in(item, ev, index, 1)
-            else:
-                wait_in(item, ev, index, None)
-                if da == 3:
-                    send(item, ev, 0, index, 0, (1, 0), (2, 0))
-                else:
-                    send(item, ev, 0, index, 1, (3, 0), (2, 0))
-            send(item, ev, 2, index, None, (0, 1), (da, 3))
-            send(item, ev, 3, index, None, (0, 3), (da, 1))
-        elif db == 2:
-            wait_in(item, ev, index, 0)
-            wait_in(item, ev, index, 1)
-        else:
-            wait_in(item, ev, index, None)
-            if db == 3:
-                send(item, ev, 0, index, 0, (0, 1), (da, 2))
-            else:
-                send(item, ev, 0, index, 1, (0, 3), (da, 2))
+        wait_in(item, ev, index)
+        if db == 0:
+            if da == 3:
+                send(item, index, 0, (1, 0), (2, 0))
+            elif da == 1:
+                send(item, index, 1, (3, 0), (2, 0))
+            send(item, index, None, (0, 1), (da, 3))
+            send(item, index, None, (0, 3), (da, 1))
+        elif db == 3:
+            send(item, index, 0, (0, 1), (da, 2))
+        elif db == 1:
+            send(item, index, 1, (0, 3), (da, 2))
         hand_over(item, ev, index)
+
+    with jax.named_scope("barrier"):
+        pl.semaphore_wait(barrier, len(others))
+    for to, there in (((1, 0), (3, 0)), ((3, 0), (1, 0))):
+        pltpu.make_async_remote_copy(
+            src_ref=wup_hbm, dst_ref=wbuf.at[0, sp], send_sem=ssem.at[UP], recv_sem=rsem.at[UP, event(*there)],
+            device_id=(slot(*to), x), device_id_type=MESH,
+        ).start()
 
     lane = lax.broadcasted_iota(jnp.int32, (64, 128), 1)
     low = lane < 64
@@ -271,12 +240,9 @@
         kvbuf[own, 384 + half * 64 : 448 + half * 64, :] = va_ref[:, tokens]
         kvbuf[own, 512 + half * 128 : 640 + half * 128, :] = vb_ref[tokens, :].astype(F32).T.astype(BF16)
 
-    with jax.named_scope("barrier"):
-        pl.semaphore_wait(barrier, len(others))
     take(KV, "a")
     take(KV, "b")
     loads[0].wait()
-    take(UP, "a")
 
     with jax.named_scope("queries"):
         gain_a = both_heads(gqa_ref)
@@ -451,7 +417,7 @@
             else:
                 part = self.parts[1 - way] if kind == 1 else self.parts[way]
                 src, dst = near.at[:, part], self.received(way).at[:, part]
-            return to_peer(way == 0, src, dst, xs.at[self.number, kind, way], xr.at[self.number, kind, way])
+            return to_peer(way == 0, src, dst, xs.at[min(self.number, 1)], xr.at[self.number, min(kind, 1), way])
 
         def start(self):
             for kind in (0, 1):
@@ -466,15 +432,14 @@
                 self.copy(2, way).start()
 
         def total(self):
-            for kind in (1, 2):
-                for way in (0, 1):
-                    self.copy(kind, way).wait_recv()
+            for way in (0, 1):
+                block = self.received(way)
+                to_peer(True, block, block, xs.at[0], xr.at[self.number, 1, way]).wait_recv()
             return self.blocks(x)[...].astype(F32) + self.received(0)[...].astype(F32) + self.received(1)[...].astype(F32)
 
-        def drain(self):
-            for kind in (0, 1, 2):
-                for way in (0, 1):
-                    self.copy(kind, way).wait_send()
+    def drain_tp(ref, sem):
+        three = ref.at[pl.ds(0, 3)]
+        to_peer(True, three, three, sem, xr.at[0, 0, 0]).wait_send()
 
     proj = TpSum(0, lambda r: pout.at[r], lambda w: phalf.at[w], lambda w: rsbuf.at[w])
     proj.start()
@@ -499,7 +464,7 @@
         block = (x + 4 - hops) % 4 if way == 0 else (x + hops) % 4
         part = halves[1 - way] if kind == 1 else halves[way]
         piece = nbuf.at[block, :, part]
-        return to_peer(way == 0, piece, piece, gs.at[kind, way], gr.at[kind, way])
+        return to_peer(way == 0, piece, piece, gs.at[0], gr.at[kind, way])
 
     for kind in (0, 1):
         for way in (0, 1):
@@ -515,91 +480,82 @@
     with jax.named_scope("upwait"):
         for ev in range(16):
             wait_partner(UP, ev, partner_slot(*ORDER[ev]))
+    with jax.named_scope("drainkv"):
+        drain(KV)
     with jax.named_scope("rowswait"):
         for kind in (1, 2):
             for way in (0, 1):
                 rows_copy(kind, way, True).wait_recv()
 
     def up(j, carry):
-        cols = pl.ds(pl.multiple_of(j * 256, 256), 256)
+        cols = pl.ds(pl.multiple_of(j * 512, 512), 512)
         rows = nbuf[...].reshape(256, 2048)
-        weights = wbuf[0, :, :, cols].reshape(2048, 256)
+        weights = wbuf[0, :, :, cols].reshape(2048, 512)
         part = jnp.maximum(jnp.dot(rows, weights, preferred_element_type=F32), 0.0)
         hidden[:, cols] = (part * part).astype(BF16)
         return carry
 
     with jax.named_scope("up"):
-        lax.fori_loop(0, 4, up, 0)
+        lax.fori_loop(0, 2, up, 0)
     for what in AMID_UP:
         take(*what)
     with jax.named_scope("up"):
-        lax.fori_loop(4, 8, up, 0)
-
-    sums = [
-        TpSum(k + 1, lambda r, k=k: dbuf.at[r, k], lambda w, k=k: dhalf.at[k, w], lambda w, k=k: frecv.at[k, w])
-        for k in range(4)
-    ]
-
-    low64 = low
+        lax.fori_loop(2, 4, up, 0)
+
+    def chunk_sum(k):
+        low_, high = CHUNKS[k]
+        cols = pl.ds(low_ * 128, (high - low_) * 128)
+        part = pl.ds(low_ * 64, (high - low_) * 64)
+        return TpSum(k + 1, lambda r: dbuf.at[r, :, cols], lambda w: dhalf.at[w, :, part], lambda w: frecv.at[w, :, cols])
+
+    sums = [chunk_sum(k) for k in range(len(CHUNKS))]
 
     def collect(k):
         total = sums[k].total()
-        for b in range(8):
+        places = ORDER[slice(*CHUNKS[k])]
+        blocks = [slot(*place) for place in places] + [partner_slot(*place) for place in places]
+        for b, block in enumerate(blocks):
             piece = total[:, (b // 2) * 128 : (b // 2) * 128 + 128]
             if b % 2 == 1:
                 piece = pltpu.roll(piece, 64, 1)
-            place = ORDER[4 * k + b % 4]
-            stage[slot(*place) if b < 4 else partner_slot(*place)] = piece
-
-    for k in range(4):
-        for what in BEFORE_DOWN[k]:
+            stage[block] = piece
+
+    def down(k):
+        first_, last_ = CHUNKS[k]
+        places = ORDER[first_:last_]
+        with jax.named_scope("dwait"):
+            for r in range(first_, last_):
+                wait_partner(DOWN, r, partner_slot(*ORDER[r]))
+        blocks = [slot(*place) for place in places] + [partner_slot(*place) for place in places]
+        part = nt_dot(hidden[...], jnp.concatenate([wbuf[1, b] for b in blocks], axis=0)).astype(BF16)
+        for r in range(4):
+            dbuf[r, :, first_ * 128 : last_ * 128] = part[r * 64 : (r + 1) * 64, :]
+        sums[k].start()
+
+    for what in TAIL:
+        if isinstance(what, tuple):
             take(*what)
-        places = ORDER[4 * k : 4 * k + 4]
-        for r in range(4):
-            wait_partner(DOWN, k * 4 + r, partner_slot(*places[r]))
-        blocks = [wbuf[1, slot(*place)] for place in places]
-        blocks += [wbuf[1, partner_slot(*place)] for place in places]
-        weights = jnp.concatenate(blocks, axis=0)
-        with jax.named_scope(f"down{k}"):
-            part = nt_dot(hidden[...], weights).astype(BF16)
-            for r in range(4):
-                dbuf[r, k] = part[r * 64 : (r + 1) * 64, :]
-        sums[k].start()
-        if k > 0:
-            with jax.named_scope(f"combine{k - 1}"):
-                sums[k - 1].combine()
-        if k > 1:
-            with jax.named_scope(f"collect{k - 2}"):
-                collect(k - 2)
-    with jax.named_scope("combine3"):
-        sums[3].combine()
-    with jax.named_scope("collect23"):
-        collect(2)
-        collect(3)
-    for pos in range(16):
-        both = jnp.where(low64, stage[2 * pos], pltpu.roll(stage[2 * pos + 1], 64, 1))
-        cols = slice(pos * 128, pos * 128 + 128)
-        out_ref[:, cols] = (midbuf[:, cols] + both).astype(BF16)
-
-    for item, ev, number, half in sends:
-        index = slot(*ORDER[ev])
-        piece = region(item, index, half)
-        pltpu.make_async_remote_copy(
-            src_ref=piece, dst_ref=piece, send_sem=ssem.at[item, ev, number], recv_sem=rsem.at[item, ev, 0],
-            device_id=(partner, x), device_id_type=MESH,
-        ).wait_send()
-    for item in (KV, UP, DOWN):
-        for ev in range(16):
-            piece = region(item, slot(*ORDER[ev]), None)
-            pltpu.make_async_remote_copy(
-                src_ref=piece, dst_ref=piece, send_sem=psend.at[item, ev], recv_sem=precv.at[item, ev],
-                device_id=(partner, x), device_id_type=MESH,
-            ).wait_send()
-    for sum_over in [proj] + sums:
-        sum_over.drain()
-    for kind in (0, 1, 2):
-        for way in (0, 1):
-            rows_copy(kind, way, False).wait_send()
+        else:
+            with jax.named_scope(what):
+                kind, k = what[:-1], int(what[-1])
+                if kind == "down":
+                    down(k)
+                elif kind == "combine":
+                    sums[k].combine()
+                else:
+                    collect(k)
+    drain(UP)
+    drain(DOWN)
+    drain_tp(pout, xs.at[0])
+    drain_tp(nbuf, gs.at[0])
+    with jax.named_scope("assemble"):
+        for pos in range(16):
+            both_halves = jnp.where(low, stage[2 * pos], pltpu.roll(stage[2 * pos + 1], 64, 1))
+            cols = slice(pos * 128, pos * 128 + 128)
+            out_ref[:, cols] = (midbuf[:, cols] + both_halves).astype(BF16)
+
+    with jax.named_scope("draintp"):
+        drain_tp(dbuf, xs.at[1])
 
 
 def local(
@@ -612,7 +568,7 @@
     dma = pltpu.SemaphoreType.DMA
     return pl.pallas_call(
         kernel,
-        out_shape=jax.ShapeDtypeStruct((64, 2048), BF16),
+        out_shape=pltpu.VMEM((64, 2048), BF16),
         in_specs=[vmem] * 13 + [anywhere] * 5,
         out_specs=vmem,
         scratch_shapes=[
@@ -633,19 +589,18 @@
             pltpu.VMEM((2, 64, 2048), BF16),
             pltpu.VMEM((4, 64, 2048), BF16),
             pltpu.VMEM((256, 2048), BF16),
-            pltpu.VMEM((4, 4, 64, 512), BF16),
-            pltpu.VMEM((4, 2, 64, 256), BF16),
-            pltpu.VMEM((4, 2, 64, 512), BF16),
+            pltpu.VMEM((4, 64, 2048), BF16),
+            pltpu.VMEM((2, 64, 1024), BF16),
+            pltpu.VMEM((2, 64, 2048), BF16),
             pltpu.VMEM((32, 64, 128), F32),
             pltpu.VMEM((64, 2048), F32),
             dma((5,)),
-            dma((3, 16, 4)),
-            dma((3, 16, 2)),
+            dma((3,)),
             dma((3, 16)),
             dma((3, 16)),
-            dma((5, 3, 2)),
-            dma((5, 3, 2)),
-            dma((3, 2)),
+            dma((2,)),
+            dma((5, 2, 2)),
+            dma((1,)),
             dma((3, 2)),
         ],
         compiler_params=pltpu.CompilerParams(

time: 87.9 us -> 82.9 us (0.943)
  Pallas kernels: 86.1 us -> 82.1 us
  local copies, waits for them, and re-layouts: 1.67 us -> 0.71 us
    pallas_call x1, Pallas kernels: 86.1 us -> 82.1 us  [local(): pl.pallas_call(kernel, out_shape=pltpu.VMEM((64, 2048), BF16), in_specs=[...]
    unnamed x1, local copies, waits for them, and re-layouts: 1.67 us -> 0.71 us
where the time goes in v3:
time: 82.9 us; the launch traced here: 82.8 us
  Pallas kernels  82.1 us (99%)
    pallas_call x1, Pallas kernels, local(): pl.pallas_call(kernel, out_shape=pltpu.VMEM((64, 2048), BF16), in_specs=[...  82.1 us

profile of v3, /device:TPU:1, one launch (start us, length us, event | category | flops | bytes accessed | tf_op | source)
XLA Modules:
  0.0 82.8 jit_solution(15422346791637520595)
XLA Ops:
  0.0 82.1 %shard_map.172 = bf16[64,2048]{1,0:T(8,128)(2,1)S(1)} custom-call(bf16[256,256]{1,0:T(8,128)(2,1)} %qa_ref.1, bf16[64,256]{1,0:T(8,128)(2,1)} %bitcast.9, bf16[64,256]{1,0:T(8,128)(2,1)} %bitcast.10, bf16[256,256]{1,0:T(8,128)(2,1)} %qb_ref.1, bf16[256,128]{1,0:T(8,128)(2,1)} %kb_ref.1, bf16[256,128]{1,0:T(8,128)(2,1)} %vb_ref.1, f32[1,64]{1,0:T(1,128)} %bitcast.12, ...), custom_call_target="tpu_custom_call" | custom-call | tf_op jit(solution)/shard_map/pallas_call | solution.py:569
  82.1 0.7 copy.20

commit v4 on v3

--- a/solution.py
+++ b/solution.py
@@ -75,13 +75,13 @@
     15: [],
     16: [(1, 3), (1, 4)],
 }
-AFTER_PROJECT = [(1, 5), (1, 6), (1, 7), "combine", (1, 8), (1, 9), (2, "a"), (2, "b"), (1, 10)]
-AFTER_SUM = [(1, 11), (1, 12), (2, 1), (2, 2), (1, 13), (1, 14), "relay", (2, 5), (2, 3), (2, 4), (1, 15)]
+AFTER_PROJECT = [(1, 5), (1, 6), (1, 7), (2, "a"), (2, "b"), "combine", (1, 8), (1, 9), (1, 10)]
+AFTER_SUM = [(1, 11), (1, 12), (2, 1), (2, 2), (1, 13), "relay", (1, 14), (2, 5), (2, 3), (2, 4), (1, 15)]
 AMID_UP = [(2, 6), (2, 7)]
-CHUNKS = ((0, 4), (4, 8), (8, 12), (12, 16))
+CHUNKS = ((0, 4), (4, 8), (8, 12), (12, 14), (14, 16))
 TAIL = [
-    "down0", (2, 8), (2, 9), "down1", (2, 11), (2, 12), "combine0", (2, 10), "down2", (2, 13), (2, 14), (2, 15), "combine1", "collect0",
-    "down3", "combine2", "collect1", "combine3", "collect2", "collect3",
+    "down0", (2, 8), (2, 9), "down1", (2, 11), (2, 12), "combine0", (2, 10), "down2", (2, 13), (2, 14), "combine1", "collect0",
+    "down3", (2, 15), "combine2", "down4", "collect1", "combine3", "collect2", "collect3", "collect4",
 ]
 
 
@@ -91,8 +91,8 @@
     resid_hbm, woa_hbm, wob_hbm, wup_hbm, wdown_hbm,
     out_ref,
     kvbuf, wbuf, wo, resid, qa, qb, s_even, s_odd, tops, acc_a, acc_b, attn,
-    pout, phalf, rsbuf, nbuf, hidden, dbuf, dhalf, frecv, stage, midbuf,
-    lsem, ssem, rsem, precv, xs, xr, gs, gr,
+    pout, phalf, rsbuf, nbuf, hidden, dbuf, dhalf, frecv, stage, midbuf, lastbuf,
+    lsem, ssem, rsem, precv, xs, xr, gs, gr, lr,
 ):
     sp = lax.axis_index("sp")
     x = lax.axis_index("tp")
@@ -111,7 +111,7 @@
 
     barrier = pltpu.get_barrier_semaphore()
     others = [(slot(1, 0), x), (slot(3, 0), x), (slot(0, 1), x), (slot(0, 3), x), (partner, x)]
-    others += [(sp, (x + d) % 4) for d in (1, 3)]
+    others += [(sp, (x + d) % 4) for d in (1, 2, 3)]
     for dev in others:
         pl.semaphore_signal(barrier, inc=1, device_id=dev, device_id_type=MESH)
 
@@ -188,13 +188,17 @@
             send(item, index, 1, (0, 3), (da, 2))
         hand_over(item, ev, index)
 
+    def own_up(half):
+        part = pl.ds(half * 32, 32)
+        for to, there in (((1, 0), (3, 0)), ((3, 0), (1, 0))):
+            pltpu.make_async_remote_copy(
+                src_ref=wup_hbm.at[part], dst_ref=wbuf.at[0, sp, part], send_sem=ssem.at[UP], recv_sem=rsem.at[UP, event(*there)],
+                device_id=(slot(*to), x), device_id_type=MESH,
+            ).start()
+
     with jax.named_scope("barrier"):
         pl.semaphore_wait(barrier, len(others))
-    for to, there in (((1, 0), (3, 0)), ((3, 0), (1, 0))):
-        pltpu.make_async_remote_copy(
-            src_ref=wup_hbm, dst_ref=wbuf.at[0, sp], send_sem=ssem.at[UP], recv_sem=rsem.at[UP, event(*there)],
-            device_id=(slot(*to), x), device_id_type=MESH,
-        ).start()
+    own_up(0)
 
     lane = lax.broadcasted_iota(jnp.int32, (64, 128), 1)
     low = lane < 64
@@ -243,6 +247,7 @@
     take(KV, "a")
     take(KV, "b")
     loads[0].wait()
+    own_up(1)
 
     with jax.named_scope("queries"):
         gain_a = both_heads(gqa_ref)
@@ -510,8 +515,23 @@
 
     sums = [chunk_sum(k) for k in range(len(CHUNKS))]
 
+    last_cols = pl.ds(CHUNKS[-1][0] * 128, (CHUNKS[-1][1] - CHUNKS[-1][0]) * 128)
+
+    def last_copy(d):
+        return pltpu.make_async_remote_copy(
+            src_ref=dbuf.at[(x + d) % 4, :, last_cols], dst_ref=lastbuf.at[d - 1], send_sem=xs.at[1], recv_sem=lr.at[d - 1],
+            device_id=(sp, (x + d) % 4), device_id_type=MESH,
+        )
+
+    def last_total():
+        total = dbuf[x, :, last_cols].astype(F32)
+        for d in (1, 3, 2):
+            last_copy(d).wait_recv()
+            total = total + lastbuf[d - 1].astype(F32)
+        return total
+
     def collect(k):
-        total = sums[k].total()
+        total = last_total() if k == len(CHUNKS) - 1 else sums[k].total()
         places = ORDER[slice(*CHUNKS[k])]
         blocks = [slot(*place) for place in places] + [partner_slot(*place) for place in places]
         for b, block in enumerate(blocks):
@@ -530,7 +550,11 @@
         part = nt_dot(hidden[...], jnp.concatenate([wbuf[1, b] for b in blocks], axis=0)).astype(BF16)
         for r in range(4):
             dbuf[r, :, first_ * 128 : last_ * 128] = part[r * 64 : (r + 1) * 64, :]
-        sums[k].start()
+        if k == len(CHUNKS) - 1:
+            for d in (2, 1, 3):
+                last_copy(d).start()
+        else:
+            sums[k].start()
 
     for what in TAIL:
         if isinstance(what, tuple):
@@ -594,6 +618,7 @@
             pltpu.VMEM((2, 64, 2048), BF16),
             pltpu.VMEM((32, 64, 128), F32),
             pltpu.VMEM((64, 2048), F32),
+            pltpu.VMEM((3, 64, 256), BF16),
             dma((5,)),
             dma((3,)),
             dma((3, 16)),
@@ -602,6 +627,7 @@
             dma((5, 2, 2)),
             dma((1,)),
             dma((3, 2)),
+            dma((3,)),
         ],
         compiler_params=pltpu.CompilerParams(
             collective_id=0, has_side_effects=True, vmem_limit_bytes=58 * 1024 * 1024

time: 82.9 us -> 79.8 us (0.963)
  Pallas kernels: 82.1 us -> 78.9 us
    pallas_call x1, Pallas kernels: 82.1 us -> 78.9 us  [local(): pl.pallas_call(kernel, out_shape=pltpu.VMEM((64, 2048), BF16), in_specs=[...]
where the time goes in v4:
time: 79.8 us; the launch traced here: 79.6 us
  Pallas kernels  78.9 us (99%)
    pallas_call x1, Pallas kernels, local(): pl.pallas_call(kernel, out_shape=pltpu.VMEM((64, 2048), BF16), in_specs=[...  78.9 us

profile of v4, /device:TPU:1, one launch (start us, length us, event | category | flops | bytes accessed | tf_op | source)
XLA Modules:
  0.0 79.6 jit_solution(17896962820556041741)
XLA Ops:
  0.0 78.9 %shard_map.172 = bf16[64,2048]{1,0:T(8,128)(2,1)S(1)} custom-call(bf16[256,256]{1,0:T(8,128)(2,1)} %qa_ref.1, bf16[64,256]{1,0:T(8,128)(2,1)} %bitcast.9, bf16[64,256]{1,0:T(8,128)(2,1)} %bitcast.10, bf16[256,256]{1,0:T(8,128)(2,1)} %qb_ref.1, bf16[256,128]{1,0:T(8,128)(2,1)} %kb_ref.1, bf16[256,128]{1,0:T(8,128)(2,1)} %vb_ref.1, f32[1,64]{1,0:T(1,128)} %bitcast.12, ...), custom_call_target="tpu_custom_call" | custom-call | tf_op jit(solution)/shard_map/pallas_call | solution.py:593
  78.9 0.7 copy.20

commit v5 on v4

--- a/solution.py
+++ b/solution.py
@@ -86,10 +86,12 @@
 
 
 def kernel(
-    qa_ref, ka_ref, va_ref, qb_ref, kb_ref, vb_ref, gqa_ref, gka_ref, gqb_ref, gkb_ref,
-    ngain_ref, rowtab_ref, coltab_ref,
+    ka_hbm, va_hbm, kb_hbm, vb_hbm, gka_hbm, gkb_hbm, rowtab_hbm, coltab_hbm,
+    qa_hbm, qb_hbm, gqa_hbm, gqb_hbm, ngain_hbm,
     resid_hbm, woa_hbm, wob_hbm, wup_hbm, wdown_hbm,
     out_ref,
+    ka_ref, va_ref, kb_ref, vb_ref, gka_ref, gkb_ref, rowtab_ref, coltab_ref,
+    qa_ref, qb_ref, gqa_ref, gqb_ref, ngain_ref,
     kvbuf, wbuf, wo, resid, qa, qb, s_even, s_odd, tops, acc_a, acc_b, attn,
     pout, phalf, rsbuf, nbuf, hidden, dbuf, dhalf, frecv, stage, midbuf, lastbuf,
     lsem, ssem, rsem, precv, xs, xr, gs, gr, lr,
@@ -122,7 +124,13 @@
         pltpu.make_async_copy(wob_hbm, wo.at[pl.ds(256, 256)], lsem.at[3]),
         pltpu.make_async_copy(resid_hbm, resid, lsem.at[4]),
     ]
-    for load in loads:
+    pairs = [
+        (ka_hbm, ka_ref), (va_hbm, va_ref), (kb_hbm, kb_ref), (vb_hbm, vb_ref), (gka_hbm, gka_ref), (gkb_hbm, gkb_ref),
+        (rowtab_hbm.at[sp], rowtab_ref), (coltab_hbm, coltab_ref),
+        (qa_hbm, qa_ref), (qb_hbm, qb_ref), (gqa_hbm, gqa_ref), (gqb_hbm, gqb_ref), (ngain_hbm, ngain_ref),
+    ]
+    inputs = [pltpu.make_async_copy(src, dst, lsem.at[5 + number]) for number, (src, dst) in enumerate(pairs)]
+    for load in inputs + loads:
         load.start()
 
     def region(item, index, half):
@@ -200,9 +208,12 @@
         pl.semaphore_wait(barrier, len(others))
     own_up(0)
 
+    with jax.named_scope("inputs"):
+        for load in inputs[0:8]:
+            load.wait()
     lane = lax.broadcasted_iota(jnp.int32, (64, 128), 1)
     low = lane < 64
-    rowtab = rowtab_ref[sp]
+    rowtab = rowtab_ref[...]
 
     def both_heads(ref):
         return jnp.concatenate([ref[...], ref[...]], axis=1)
@@ -250,6 +261,8 @@
     own_up(1)
 
     with jax.named_scope("queries"):
+        for load in inputs[8:]:
+            load.wait()
         gain_a = both_heads(gqa_ref)
         for g in range(2):
             lanes = slice(g * 128, g * 128 + 128)
@@ -593,9 +606,22 @@
     return pl.pallas_call(
         kernel,
         out_shape=pltpu.VMEM((64, 2048), BF16),
-        in_specs=[vmem] * 13 + [anywhere] * 5,
+        in_specs=[anywhere] * 18,
         out_specs=vmem,
         scratch_shapes=[
+            pltpu.VMEM((64, 256), BF16),
+            pltpu.VMEM((64, 256), BF16),
+            pltpu.VMEM((256, 128), BF16),
+            pltpu.VMEM((256, 128), BF16),
+            pltpu.VMEM((1, 64), F32),
+            pltpu.VMEM((1, 128), F32),
+            pltpu.VMEM((16, 128), F32),
+            pltpu.VMEM((4, 64, 128), F32),
+            pltpu.VMEM((256, 256), BF16),
+            pltpu.VMEM((256, 256), BF16),
+            pltpu.VMEM((1, 64), F32),
+            pltpu.VMEM((1, 128), F32),
+            pltpu.VMEM((1, 2048), F32),
             pltpu.VMEM((32, 768, 128), BF16),
             pltpu.VMEM((2, 32, 64, 2048), BF16),
             pltpu.VMEM((512, 2048), BF16),
@@ -619,7 +645,7 @@
             pltpu.VMEM((32, 64, 128), F32),
             pltpu.VMEM((64, 2048), F32),
             pltpu.VMEM((3, 64, 256), BF16),
-            dma((5,)),
+            dma((18,)),
             dma((3,)),
             dma((3, 16)),
             dma((3, 16)),
@@ -633,9 +659,9 @@
             collective_id=0, has_side_effects=True, vmem_limit_bytes=58 * 1024 * 1024
         ),
     )(
-        query_a, key_a.T, value_a.T, query_b, key_b, value_b,
-        gain_qa.reshape(1, -1), gain_ka.reshape(1, -1), gain_qb.reshape(1, -1), gain_kb.reshape(1, -1),
-        norm_gain.reshape(1, -1), jnp.asarray(rowtab), jnp.asarray(coltab),
+        key_a.T, value_a.T, key_b, value_b, gain_ka.reshape(1, -1), gain_kb.reshape(1, -1),
+        jnp.asarray(rowtab), jnp.asarray(coltab),
+        query_a, query_b, gain_qa.reshape(1, -1), gain_qb.reshape(1, -1), norm_gain.reshape(1, -1),
         resid, w_out_a, w_out_b, w_up, w_down.T,
     )
 

time: 79.8 us -> 78.6 us (0.985)
  Pallas kernels: 78.9 us -> 77.8 us
    pallas_call x1, Pallas kernels: 78.9 us -> 77.8 us  [local(): pl.pallas_call(kernel, out_shape=pltpu.VMEM((64, 2048), BF16), in_specs=[...]
where the time goes in v5:
time: 78.6 us; the launch traced here: 78.5 us
  Pallas kernels  77.8 us (99%)
    pallas_call x1, Pallas kernels, local(): pl.pallas_call(kernel, out_shape=pltpu.VMEM((64, 2048), BF16), in_specs=[...  77.8 us

profile of v5, /device:TPU:1, one launch (start us, length us, event | category | flops | bytes accessed | tf_op | source)
XLA Modules:
  0.0 78.5 jit_solution(10980114476576295088)
XLA Ops:
  0.0 77.8 %shard_map.172 = bf16[64,2048]{1,0:T(8,128)(2,1)S(1)} custom-call(bf16[64,256]{1,0:T(8,128)(2,1)} %bitcast.9, bf16[64,256]{1,0:T(8,128)(2,1)} %bitcast.10, bf16[256,128]{1,0:T(8,128)(2,1)} %kb_hbm.1, bf16[256,128]{1,0:T(8,128)(2,1)} %vb_hbm.1, f32[1,64]{1,0:T(1,128)} %bitcast.12, f32[1,128]{1,0:T(1,128)} %bitcast.13, ...), custom_call_target="tpu_custom_call" | custom-call | tf_op jit(solution)/shard_map/pallas_call | solution.py:606
  77.8 0.7 copy.20

commit v6 on v5

--- a/solution.py
+++ b/solution.py
@@ -196,8 +196,8 @@
             send(item, index, 1, (0, 3), (da, 2))
         hand_over(item, ev, index)
 
-    def own_up(half):
-        part = pl.ds(half * 32, 32)
+    def own_up(start, count):
+        part = pl.ds(start, count)
         for to, there in (((1, 0), (3, 0)), ((3, 0), (1, 0))):
             pltpu.make_async_remote_copy(
                 src_ref=wup_hbm.at[part], dst_ref=wbuf.at[0, sp, part], send_sem=ssem.at[UP], recv_sem=rsem.at[UP, event(*there)],
@@ -206,7 +206,7 @@
 
     with jax.named_scope("barrier"):
         pl.semaphore_wait(barrier, len(others))
-    own_up(0)
+    own_up(0, 16)
 
     with jax.named_scope("inputs"):
         for load in inputs[0:8]:
@@ -258,7 +258,7 @@
     take(KV, "a")
     take(KV, "b")
     loads[0].wait()
-    own_up(1)
+    own_up(16, 48)
 
     with jax.named_scope("queries"):
         for load in inputs[8:]:

time: 78.6 us -> 78.8 us (level)
  no operation moved by 1% of the time
where the time goes in v6:
time: 78.8 us; the launch traced here: 78.7 us
  Pallas kernels  78 us (99%)
    pallas_call x1, Pallas kernels, local(): pl.pallas_call(kernel, out_shape=pltpu.VMEM((64, 2048), BF16), in_specs=[...  78 us

profile of v6, /device:TPU:1, one launch (start us, length us, event | category | flops | bytes accessed | tf_op | source)
XLA Modules:
  0.0 78.7 jit_solution(14238879467189529167)
XLA Ops:
  0.0 78.0 %shard_map.172 = bf16[64,2048]{1,0:T(8,128)(2,1)S(1)} custom-call(bf16[64,256]{1,0:T(8,128)(2,1)} %bitcast.9, bf16[64,256]{1,0:T(8,128)(2,1)} %bitcast.10, bf16[256,128]{1,0:T(8,128)(2,1)} %kb_hbm.1, bf16[256,128]{1,0:T(8,128)(2,1)} %vb_hbm.1, f32[1,64]{1,0:T(1,128)} %bitcast.12, f32[1,128]{1,0:T(1,128)} %bitcast.13, ...), custom_call_target="tpu_custom_call" | custom-call | tf_op jit(solution)/shard_map/pallas_call | solution.py:606
  78.0 0.7 copy.20
